TPU v7x, 32 devices: a whole 2x2x4 slice. The times are simulated.
32 devices in a mesh: ep: 4 (over y, x), tp: 8 (over z, core).
Axes of the slice: x: 2, y: 2, z: 4, core: 2. Of those that a mesh axis runs over, the one named last changes fastest.
Arguments:
- receptance: bfloat16 [4096, 1024], P('ep', 'tp'), may hold values from -6 to 6
- key_in: bfloat16 [4096, 1024], P('ep', 'tp'), may hold values from -6 to 6
- payload_vectors: bfloat16 [4096, 1024], P('ep', 'tp'), may hold values from -6 to 6
- decay_in: bfloat16 [4096, 1024], P('ep', 'tp'), may hold values from -30 to 3
- rate_in: bfloat16 [4096, 1024], P('ep', 'tp'), may hold values from -30 to 6
- gate_in: bfloat16 [4096, 1024], P('ep', 'tp'), may hold values from -6 to 6
- norm_gain: float32 [1024], P('tp'), may hold values from 0.1 to 1.9
- out_weight: bfloat16 [1024, 2048], P('tp'), may hold values from -0.1875 to 0.1875
- moe_in: bfloat16 [4096, 2048], P(('ep', 'tp')), may hold values from -6 to 6
- moe_gain: float32 [2048], replicated, may hold values from 0.1 to 1.9
- routes: int32 [4096, 2], P(('ep', 'tp')), may hold values from 0 to 7, all different within a row; in each aligned block of 128 rows (0 to 127, 128 to 255, ...) at most 48 rows name the same one
- route_weights: float32 [4096, 2], P(('ep', 'tp')), may hold values from 0.2 to 1
- expert_gate: bfloat16 [8, 2048, 512], P('ep', None, 'tp'), may hold values from -0.125 to 0.125
- expert_up: bfloat16 [8, 2048, 512], P('ep', None, 'tp'), may hold values from -0.125 to 0.125
- expert_down: bfloat16 [8, 2048, 512], P('ep', None, 'tp'), may hold values from -0.25 to 0.25
- shared_gate: bfloat16 [2048, 512], replicated, may hold values from -0.125 to 0.125
- shared_up: bfloat16 [2048, 512], replicated, may hold values from -0.125 to 0.125
- shared_down: bfloat16 [512, 2048], replicated, may hold values from -0.25 to 0.25
Outputs:
- mixed: bfloat16 [4096, 2048], P(('ep', 'tp'))
- moe_out: bfloat16 [4096, 2048], P(('ep', 'tp'))
Inputs may be any that keep to these rules, and one draw needn't show every extreme that they name: `routes`: each token names 2 different experts; within the rows of one device no expert is named more than 48 times, a bound that some block reaches there.
All inputs are finite; a program needn't handle non-finite values.
Results may differ from a plain program's by a relative error of at most 0.019.
Values may be sent and summed in bfloat16 or wider, within the bound.
A program may use at most 128 MiB of HBM per device.

v0:
```python
import functools

import jax
import jax.numpy as jnp
from jax import lax
from jax.experimental import pallas as pl
from jax.experimental.pallas import tpu as pltpu
from jax.sharding import PartitionSpec as P

HEAD_DIM = 64
BLOCK = 64


def dims(form):
    return {"nn": ((1,), (0,)), "nt": ((1,), (1,)), "tn": ((0,), (0,))}[form]


def mm1(left, right, form="nn"):
    return lax.dot_general(
        left.astype(jnp.bfloat16),
        right.astype(jnp.bfloat16),
        (dims(form), ((), ())),
        preferred_element_type=jnp.float32,
    )


def mm3(left, right, form="nn"):
    lh, rh = left.astype(jnp.bfloat16), right.astype(jnp.bfloat16)
    ll = (left - lh.astype(jnp.float32)).astype(jnp.bfloat16)
    rl = (right - rh.astype(jnp.float32)).astype(jnp.bfloat16)
    return mm1(lh, rh, form) + (mm1(lh, rl, form) + mm1(ll, rh, form))


mm_g = mm3
mm_inv = mm3
mm_q = mm3
mm_out = mm3
mm_car = mm3
mm_scan = mm3


def head_masks(rows, width):
    lane = lax.broadcasted_iota(jnp.int32, (rows, width), 1)
    return lane < HEAD_DIM


def stacked(x):
    first = head_masks(*x.shape)
    return jnp.concatenate([jnp.where(first, x, 0.0), jnp.where(first, 0.0, x)], axis=0)


def per_head_sum(x):
    first = head_masks(*x.shape)
    one = jnp.sum(jnp.where(first, x, 0.0), axis=-1, keepdims=True)
    both = jnp.sum(jnp.where(first, 0.0, x), axis=-1, keepdims=True)
    return jnp.where(first, one, both)


def sigmoid(x):
    return 1.0 / (1.0 + jnp.exp(-x))


def local_block(r_in, k_in, v_in, d_in, b_in):
    f32 = jnp.float32
    keys = k_in.astype(f32)
    unit = keys * lax.rsqrt(per_head_sum(keys * keys) + 1e-06)
    log_decay = sigmoid(d_in.astype(f32)) * -0.6065306597126334
    tri_row = lax.broadcasted_iota(jnp.int32, (BLOCK, 3 * BLOCK), 0)
    tri_col = lax.broadcasted_iota(jnp.int32, (BLOCK, 3 * BLOCK), 1) % BLOCK
    tri = jnp.where(tri_col <= tri_row, 1.0, 0.0).astype(jnp.bfloat16)
    hi = log_decay.astype(jnp.bfloat16)
    rest = log_decay - hi.astype(f32)
    mid = rest.astype(jnp.bfloat16)
    low = (rest - mid.astype(f32)).astype(jnp.bfloat16)
    cumul = mm1(tri, jnp.concatenate([hi, mid, low], axis=0))
    end_scale = jnp.exp(cumul[BLOCK - 1 :, :])
    shrink = jnp.exp(-cumul)
    query2 = stacked(r_in.astype(f32) * jnp.exp(cumul))
    alpha2 = stacked(-unit * jnp.exp(cumul - log_decay))
    key_grow = keys * shrink
    beta_grow = unit * sigmoid(b_in.astype(f32)) * shrink
    values2 = stacked(v_in.astype(f32))
    two = 2 * BLOCK
    grams = mm_g(
        jnp.concatenate([alpha2, query2], axis=0),
        jnp.concatenate([beta_grow, beta_grow, key_grow, key_grow], axis=0),
        "nt",
    )
    row = lax.broadcasted_iota(jnp.int32, (two, two), 0)
    col = lax.broadcasted_iota(jnp.int32, (two, two), 1)
    same = row // BLOCK == col // BLOCK
    strict = same & (col < row)
    inclusive = same & (col <= row)
    couple = jnp.where(strict, grams[:two, :two], 0.0)
    insert = jnp.where(strict, grams[:two, two:], 0.0)
    read_beta = jnp.where(inclusive, grams[two:, :two], 0.0)
    read_key = jnp.where(inclusive, grams[two:, two:], 0.0)
    size = 8
    near = jnp.where(row // size == col // size, couple, 0.0)
    inverse = jnp.where(row == col, 1.0, 0.0) + near
    power = mm_inv(near, near)
    both = mm_inv(jnp.concatenate([inverse, power], axis=0), power)
    inverse = inverse + both[:two]
    inverse = inverse + mm_inv(inverse, both[two:])
    while size < BLOCK:
        wide = 2 * size
        off = jnp.where(
            (row // wide == col // wide) & (row // size != col // size), couple, 0.0
        )
        inverse = inverse + mm_inv(inverse, mm_inv(off, inverse))
        size = wide
    inserted = mm_q(insert, values2)
    qz = mm_q(inverse, jnp.concatenate([alpha2, inserted], axis=1))
    lower = jnp.concatenate([jnp.zeros_like(values2), values2], axis=1)
    stack = jnp.concatenate([qz, lower], axis=0)
    reads = mm_out(jnp.concatenate([read_beta, read_key], axis=1), stack)
    query_bar = query2 + reads[:, :two]
    local_out = reads[:, two:]
    ends = jnp.concatenate([stacked(beta_grow * end_scale), stacked(key_grow * end_scale)], axis=0)
    maps = mm_car(stack, ends, "tn")
    return query_bar, local_out, maps, end_scale


def mixer_kernel(
    unroll,
    groups,
    ring,
    r_ref,
    k_ref,
    v_ref,
    d_ref,
    b_ref,
    gate_ref,
    gain_ref,
    weight_ref,
    slab_ref,
    token_ref,
    whole_ref,
    project_ref,
    state,
    qp_ref,
    lo_ref,
    rows_ref,
    totals,
    ring_send,
    ring_recv,
    pair_send,
    pair_recv,
    ep_send,
    ep_recv,
    row_send,
    row_recv,
    own_sem,
    slab_ring_send,
    slab_ring_recv,
    slab_send,
    slab_recv,
):
    two = 2 * BLOCK
    peers = 2 * ring
    here, mine = lax.axis_index("ep"), lax.axis_index("tp")
    depth, core = mine // 2, mine % 2
    partner = depth * 2 + 1 - core
    after = (depth + 1) % ring * 2 + core
    before = (depth + ring - 1) % ring * 2 + core
    chunks, height = weight_ref.shape[0], weight_ref.shape[1]
    kinds = chunks // 2
    span = peers * height
    tokens = token_ref.shape[0]
    MESH = pl.DeviceIdType.MESH

    def place(chunk, origin):
        base = chunk * span + origin * height
        return whole_ref.at[pl.ds(pl.multiple_of(base, height), height), :]

    def ring_copy(source, chunk, origin, step, target):
        return pltpu.make_async_remote_copy(
            src_ref=source,
            dst_ref=place(chunk, origin),
            send_sem=ring_send.at[chunk, step],
            recv_sem=ring_recv.at[chunk, step],
            device_id={"tp": target},
            device_id_type=MESH,
        )

    def pair_copy(source, chunk, origin, step):
        return pltpu.make_async_remote_copy(
            src_ref=source,
            dst_ref=place(chunk, origin),
            send_sem=pair_send.at[chunk, step],
            recv_sem=pair_recv.at[chunk, step],
            device_id={"tp": partner},
            device_id_type=MESH,
        )

    half, columns = slab_ref.shape[0] // 2, slab_ref.shape[1]

    def slab_place(way, origin):
        return project_ref.at[
            pl.ds(pl.multiple_of(origin * 2 * half + way * half, half), half),
            pl.ds(pl.multiple_of(here * columns, columns), columns),
        ]

    def slab_ring(source, way, origin, step):
        return pltpu.make_async_remote_copy(
            src_ref=source,
            dst_ref=slab_place(way, origin),
            send_sem=slab_ring_send.at[way, step],
            recv_sem=slab_ring_recv.at[way, step],
            device_id={"tp": (after, before)[way]},
            device_id_type=MESH,
        )

    def slab_copies(source, way, origin, step):
        for q in range(groups):
            for flip in (0, 1):
                if q or flip:
                    yield pltpu.make_async_remote_copy(
                        src_ref=source,
                        dst_ref=slab_place(way, origin),
                        send_sem=slab_send.at[way, step, q, flip],
                        recv_sem=slab_recv.at[way, step, q, flip],
                        device_id={
                            "ep": (here + q) % groups,
                            "tp": (mine, partner)[flip],
                        },
                        device_id_type=MESH,
                    )

    def slab_own(way):
        return pltpu.make_async_copy(
            slab_ref.at[pl.ds(way * half, half), :],
            slab_place(way, mine),
            own_sem.at[chunks + 1 + way],
        )

    def slab_relay(hop, carry):
        for way in (0, 1):
            shift = ring - hop if way == 0 else hop
            origin = (depth + shift) % ring * 2 + core
            block = slab_place(way, origin)
            slab_ring(block, way, origin, hop - 1).wait_recv()

            @pl.when(hop < ring - 1)
            def _():
                slab_ring(block, way, origin, hop).start()

            for copy in slab_copies(block, way, origin, hop):
                copy.start()
        return carry

    def own_copy(chunk):
        return pltpu.make_async_copy(
            weight_ref.at[chunk], place(chunk, mine), own_sem.at[chunk]
        )

    barrier = pltpu.get_barrier_semaphore()
    for q in range(1, peers):
        pl.semaphore_signal(
            barrier, inc=1, device_id={"tp": (mine + q) % peers}, device_id_type=MESH
        )
    for q in range(1, groups):
        pl.semaphore_signal(
            barrier, inc=1, device_id={"ep": (here + q) % groups}, device_id_type=MESH
        )
    for q in range(1, groups):
        pl.semaphore_signal(
            barrier,
            inc=1,
            device_id={"ep": (here + q) % groups, "tp": partner},
            device_id_type=MESH,
        )
    pl.semaphore_wait(barrier, peers + 2 * groups - 3)
    for way in (0, 1):
        piece = slab_ref.at[pl.ds(way * half, half), :]
        slab_ring(piece, way, mine, 0).start()
        slab_own(way).start()
        for copy in slab_copies(piece, way, mine, 0):
            copy.start()

    def begin(kind, carry):
        for way, target in ((0, after), (1, before)):
            chunk = kind * 2 + way
            ring_copy(weight_ref.at[chunk], chunk, mine, 0, target).start()
            pair_copy(weight_ref.at[chunk], chunk, mine, 0).start()
            own_copy(chunk).start()
        return carry

    lax.fori_loop(0, kinds, begin, 0)

    def relay(k, carry):
        hop, kind = k // kinds + 1, k % kinds
        for way, target in ((0, after), (1, before)):
            chunk = kind * 2 + way
            shift = ring - hop if way == 0 else hop
            origin = (depth + shift) % ring * 2 + core
            block = place(chunk, origin)
            ring_copy(block, chunk, origin, hop - 1, target).wait_recv()

            @pl.when(hop < ring - 1)
            def _():
                ring_copy(block, chunk, origin, hop, target).start()

            pair_copy(block, chunk, origin, hop).start()
        return carry

    row = lax.broadcasted_iota(jnp.int32, (2 * two, two), 0)
    col = lax.broadcasted_iota(jnp.int32, (2 * two, two), 1)
    state[...] = jnp.where(row == col, 1.0, 0.0)
    turns = r_ref.shape[0] // (BLOCK * unroll)
    relays = (ring - 1) * kinds
    each = 2
    inside = min(turns, relays // each)

    def turn(step, carry):
        parts = []
        for u in range(unroll):
            rows = pl.ds(pl.multiple_of((step * unroll + u) * BLOCK, BLOCK), BLOCK)
            parts.append(
                local_block(
                    r_ref[rows, :], k_ref[rows, :], v_ref[rows, :], d_ref[rows, :], b_ref[rows, :]
                )
            )
        now = state[...]
        for u, (query_bar, local_out, maps, end_scale) in enumerate(parts):
            rows = pl.ds(pl.multiple_of((step * unroll + u) * BLOCK, BLOCK), BLOCK)
            out = mm_scan(query_bar, now, "nt")
            qp_ref[rows, :] = out[:BLOCK, :two] + out[BLOCK:, :two]
            lo = out[:, two:] + local_out
            lo_ref[rows, :] = lo[:BLOCK] + lo[BLOCK:]
            moved = mm_scan(now, maps[:two]) + now * end_scale
            now = jnp.concatenate([moved[:two], moved[two:] + maps[two:]], axis=0)
        state[...] = now

        @pl.when((step >= 1) & (step < ring))
        def _():
            slab_relay(step, 0)

        @pl.when(step < inside)
        def _():
            lax.fori_loop(step * each, (step + 1) * each, relay, 0)

        return carry

    lax.fori_loop(0, turns, turn, 0)

    carry_map, source_map = state[:two, :], state[two:, :]
    totals[here, 0] = (carry_map[:BLOCK] + carry_map[BLOCK:]).astype(totals.dtype)
    totals[here, 1] = (source_map[:BLOCK] + source_map[BLOCK:]).astype(totals.dtype)

    def ep_copy(q, slot):
        return pltpu.make_async_remote_copy(
            src_ref=totals.at[slot],
            dst_ref=totals.at[slot],
            send_sem=ep_send.at[q],
            recv_sem=ep_recv.at[q],
            device_id={"ep": (here + q) % groups},
            device_id_type=MESH,
        )

    for q in range(1, groups):
        ep_copy(q, here).start()
    for q in range(1, groups):
        ep_copy(q, (here + groups - q) % groups).wait_recv()

    def enter(k, entry):
        carry = stacked(totals[k, 0].astype(jnp.float32))
        source = stacked(totals[k, 1].astype(jnp.float32))
        reached = jnp.where(k < here, 1.0, 0.0)
        return entry + reached * (mm3(entry, carry) + source - entry)

    entry = lax.fori_loop(0, groups, enter, jnp.zeros((two, two), jnp.float32))
    entry = entry.astype(jnp.float32)

    def row_copy(q, target, source):
        return pltpu.make_async_remote_copy(
            src_ref=rows_ref.at[pl.ds(pl.multiple_of(target * tokens, tokens), tokens), :],
            dst_ref=token_ref.at[:, pl.ds(pl.multiple_of(source * two, two), two)],
            send_sem=row_send.at[q],
            recv_sem=row_recv.at[q],
            device_id={"tp": target},
            device_id_type=MESH,
        )

    def finish(rows):
        recur = mm3(qp_ref[rows, :], entry, "nt") + lo_ref[rows, :]
        centered = recur - per_head_sum(recur) * (1.0 / HEAD_DIM)
        spread = per_head_sum(centered * centered) * (1.0 / HEAD_DIM)
        normed = centered * lax.rsqrt(spread + 0.00064)
        gated = normed * gain_ref[...] * sigmoid(gate_ref[rows, :].astype(jnp.float32))
        rows_ref[rows, :] = gated.astype(rows_ref.dtype)

    def finish_turn(q, carry):
        target = (mine + q) % peers
        finish(pl.ds(pl.multiple_of(target * tokens, tokens), tokens))
        return carry

    lax.fori_loop(0, peers, finish_turn, 0)
    own = rows_ref.at[pl.ds(pl.multiple_of(mine * tokens, tokens), tokens), :]
    own_rows = pltpu.make_async_copy(
        own, token_ref.at[:, pl.ds(pl.multiple_of(mine * two, two), two)], own_sem.at[chunks]
    )
    own_rows.start()

    def row_start(q, carry):
        row_copy(q, (mine + q) % peers, mine).start()
        return carry

    lax.fori_loop(1, peers, row_start, 0)

    lax.fori_loop(min(turns, ring), ring, slab_relay, 0)
    lax.fori_loop(inside * each, relays, relay, 0)

    def slab_close(hop, carry):
        for way in (0, 1):
            piece = slab_ref.at[pl.ds(way * half, half), :]
            for copy in slab_copies(piece, way, mine, hop):
                copy.wait()

            @pl.when(hop < ring - 1)
            def _():
                slab_ring(piece, way, mine, hop).wait_send()

        return carry

    lax.fori_loop(0, ring, slab_close, 0)
    slab_own(0).wait()
    slab_own(1).wait()

    def close(chunk, carry):
        own_copy(chunk).wait()

        def shut(hop, inner):
            pair_copy(weight_ref.at[chunk], chunk, mine, hop).wait()
            return inner

        def shut_ring(hop, inner):
            ring_copy(weight_ref.at[chunk], chunk, mine, hop, after).wait_send()
            return inner

        lax.fori_loop(0, ring, shut, 0)
        lax.fori_loop(0, ring - 1, shut_ring, 0)
        return carry

    lax.fori_loop(0, chunks, close, 0)
    own_rows.wait()

    def row_end(q, carry):
        row_copy(q, (mine + q) % peers, (mine + peers - q) % peers).wait()
        return carry

    lax.fori_loop(1, peers, row_end, 0)
    for q in range(1, groups):
        ep_copy(q, here).wait_send()


def mixer_and_weights(
    receptance, key_in, payload_vectors, decay_in, rate_in, gate_in, norm_gain, weights, out_weight
):
    length, channels = receptance.shape
    groups, peers = lax.axis_size("ep"), lax.axis_size("tp")
    ring = peers // 2
    wide = 2 * HEAD_DIM
    spare = wide - channels
    pad = lambda x: jnp.pad(x, ((0, 0),) * (x.ndim - 1) + ((0, spare),)) if spare else x
    chunks, height, width = weights.shape
    vmem = pl.BlockSpec(memory_space=pltpu.VMEM)
    dma = pltpu.SemaphoreType.DMA
    columns = width // groups
    slab = lax.dynamic_slice_in_dim(out_weight, lax.axis_index("ep") * columns, columns, axis=1)
    tokens, whole, project = pl.pallas_call(
        functools.partial(mixer_kernel, 4, groups, ring),
        out_shape=(
            jax.ShapeDtypeStruct((length // peers, peers * wide), jnp.bfloat16),
            jax.ShapeDtypeStruct((chunks * peers * height, width), jnp.bfloat16),
            jax.ShapeDtypeStruct((peers * out_weight.shape[0], width), jnp.bfloat16),
        ),
        in_specs=[vmem] * 9,
        out_specs=(vmem, pl.BlockSpec(memory_space=pl.ANY), pl.BlockSpec(memory_space=pl.ANY)),
        scratch_shapes=[
            pltpu.VMEM((2 * wide, wide), jnp.float32),
            pltpu.VMEM((length, wide), jnp.float32),
            pltpu.VMEM((length, wide), jnp.float32),
            pltpu.VMEM((length, wide), jnp.bfloat16),
            pltpu.VMEM((groups, 2, HEAD_DIM, wide), jnp.bfloat16),
            dma((chunks, ring)),
            dma((chunks, ring)),
            dma((chunks, ring)),
            dma((chunks, ring)),
            dma((groups,)),
            dma((groups,)),
            dma((peers,)),
            dma((peers,)),
            dma((chunks + 3,)),
            dma((2, ring)),
            dma((2, ring)),
            dma((2, ring, groups, 2)),
            dma((2, ring, groups, 2)),
        ],
        compiler_params=pltpu.CompilerParams(collective_id=0, has_side_effects=True),
        cost_estimate=pl.CostEstimate(
            flops=2 * length * wide * wide * 200, bytes_accessed=32 << 20, transcendentals=0
        ),
    )(
        pad(receptance),
        pad(key_in),
        pad(payload_vectors),
        pad(decay_in),
        pad(rate_in),
        pad(gate_in),
        pad(norm_gain).reshape(1, wide),
        weights,
        slab,
    )
    if spare:
        tokens = tokens.reshape(-1, peers, wide)[:, :, :channels].reshape(-1, peers * channels)
    return tokens, whole, project


def silu(x):
    return x / (1.0 + jnp.exp(-x))


def ffn_kernel(x_ref, gate_ref, up_ref, down_ref, out_ref):
    groups, slots, width = x_ref.shape[0], x_ref.shape[2], x_ref.shape[3]
    x = x_ref[...].reshape(groups * slots, width)
    nt = (((1,), (1,)), ((), ()))
    gate = lax.dot_general(x, gate_ref[0], nt, preferred_element_type=jnp.float32)
    upper = lax.dot_general(x, up_ref[0], nt, preferred_element_type=jnp.float32)
    hidden = (silu(gate) * upper).astype(jnp.bfloat16)
    out = jnp.dot(hidden, down_ref[0], preferred_element_type=jnp.float32)
    out_ref[...] = out.astype(jnp.bfloat16).reshape(groups, 1, slots, width)


def expert_layer(
    moe_in,
    moe_gain,
    routes,
    route_weights,
    local_count,
    whole,
    shared_gate,
    shared_up,
    shared_down,
):
    tokens, width = moe_in.shape
    top_count = routes.shape[1]
    groups = lax.axis_size("ep")
    experts = local_count * groups
    slots = max(2, 3 * tokens * top_count // (2 * experts))
    slots = -(-slots // 16) * 16
    values = moe_in.astype(jnp.float32)
    centered = values - jnp.mean(values, -1, keepdims=True)
    rescaled_input = (
        centered * lax.rsqrt(jnp.mean(centered * centered, -1, keepdims=True) + 1e-05) * moe_gain
    ).astype(jnp.bfloat16)
    flat = routes.reshape(-1)
    picks = (flat[:, None] == jnp.arange(experts, dtype=jnp.int32)[None, :]).astype(jnp.int32)
    earlier = jnp.cumsum(picks, axis=0) - picks
    rank = jnp.sum(earlier * picks, axis=1)
    slot_index = (flat * slots + rank).reshape(tokens, top_count)
    total_slots = experts * slots
    slot_row = jnp.arange(total_slots, dtype=jnp.int32)[None, :]
    match = [slot_index[:, k : k + 1] == slot_row for k in range(top_count)]
    chosen = functools.reduce(jnp.logical_or, match).astype(jnp.bfloat16)
    outgoing = lax.dot_general(
        chosen, rescaled_input, (((0,), (0,)), ((), ())), preferred_element_type=jnp.float32
    ).astype(jnp.bfloat16)
    outgoing = outgoing.reshape(groups, local_count * slots, width)
    arrived = lax.all_to_all(outgoing, "ep", split_axis=0, concat_axis=0, tiled=True).reshape(
        groups, local_count, slots, width
    )
    shared_gate_out = jnp.dot(rescaled_input, shared_gate, preferred_element_type=jnp.float32)
    shared_up_out = jnp.dot(rescaled_input, shared_up, preferred_element_type=jnp.float32)
    shared_hidden = (jax.nn.silu(shared_gate_out) * shared_up_out).astype(jnp.bfloat16)
    shared_term = jnp.dot(shared_hidden, shared_down, preferred_element_type=jnp.float32)
    span = whole.shape[1]
    block = (groups, 1, slots, width)
    results = pl.pallas_call(
        ffn_kernel,
        grid=(local_count,),
        out_shape=jax.ShapeDtypeStruct((groups, local_count, slots, width), jnp.bfloat16),
        in_specs=[pl.BlockSpec(block, lambda e: (0, e, 0, 0))]
        + [
            pl.BlockSpec((1, span, width), functools.partial(lambda k, e: (k + e, 0, 0), k))
            for k in (0, local_count, 2 * local_count)
        ],
        out_specs=pl.BlockSpec(block, lambda e: (0, e, 0, 0)),
        cost_estimate=pl.CostEstimate(
            flops=6 * total_slots * width * span, bytes_accessed=16 << 20, transcendentals=0
        ),
    )(arrived, whole, whole, whole)
    sending = results.reshape(groups, local_count * slots, width)
    returned = lax.all_to_all(sending, "ep", split_axis=0, concat_axis=0, tiled=True).reshape(
        total_slots, width
    )
    share = 2.5 * route_weights / jnp.sum(route_weights, -1, keepdims=True)
    spread = sum(jnp.where(match[k], share[:, k : k + 1], 0.0) for k in range(top_count))
    high = spread.astype(jnp.bfloat16)
    low = (spread - high.astype(jnp.float32)).astype(jnp.bfloat16)
    routed = jnp.dot(high, returned, preferred_element_type=jnp.float32) + jnp.dot(
        low, returned, preferred_element_type=jnp.float32
    )
    return (shared_term + routed).astype(jnp.bfloat16)


def project_kernel(rows_ref, weight_ref, out_ref):
    out_ref[...] = jnp.dot(
        rows_ref[...], weight_ref[...], preferred_element_type=jnp.float32
    ).astype(out_ref.dtype)


def shards(
    receptance,
    key_in,
    payload_vectors,
    decay_in,
    rate_in,
    gate_in,
    norm_gain,
    out_weight,
    moe_in,
    moe_gain,
    routes,
    route_weights,
    expert_gate,
    expert_up,
    expert_down,
    shared_gate,
    shared_up,
    shared_down,
):
    local_count, width, part = expert_gate.shape
    weights = jnp.concatenate(
        [jnp.swapaxes(w, 1, 2) for w in (expert_gate, expert_up, expert_down)], axis=0
    )
    token_rows, whole, project = mixer_and_weights(
        receptance,
        key_in,
        payload_vectors,
        decay_in,
        rate_in,
        gate_in,
        norm_gain,
        weights,
        out_weight,
    )
    mixed = pl.pallas_call(
        project_kernel,
        grid=(2,),
        out_shape=jax.ShapeDtypeStruct((token_rows.shape[0], width), jnp.bfloat16),
        in_specs=[
            pl.BlockSpec(token_rows.shape, lambda n: (0, 0)),
            pl.BlockSpec((token_rows.shape[1], width // 2), lambda n: (0, n)),
        ],
        out_specs=pl.BlockSpec((token_rows.shape[0], width // 2), lambda n: (0, n)),
        cost_estimate=pl.CostEstimate(
            flops=2 * token_rows.size * width, bytes_accessed=5 << 20, transcendentals=0
        ),
    )(token_rows, project)
    moe_out = expert_layer(
        moe_in,
        moe_gain,
        routes,
        route_weights,
        local_count,
        whole.reshape(3 * local_count, -1, width),
        shared_gate,
        shared_up,
        shared_down,
    )
    return (mixed, moe_out)


def solution(mesh):
    placed = (
        P("ep", "tp"),
        P("ep", "tp"),
        P("ep", "tp"),
        P("ep", "tp"),
        P("ep", "tp"),
        P("ep", "tp"),
        P("tp"),
        P("tp", None),
        P(("ep", "tp"), None),
        P(),
        P(("ep", "tp"), None),
        P(("ep", "tp"), None),
        P("ep", None, "tp"),
        P("ep", None, "tp"),
        P("ep", None, "tp"),
        P(),
        P(),
        P(),
    )
    return jax.shard_map(
        shards,
        mesh=mesh,
        in_specs=placed,
        out_specs=(P(("ep", "tp"), None), P(("ep", "tp"), None)),
        check_vma=False,
    )
```

profile of v0, /device:TPU:0, one launch (start us, length us, event | category | flops | bytes accessed | tf_op | source)
XLA Modules:
  0.0 180.2 jit_solution(13689036814063547377)
XLA Ops:
  0.6 0.0 copy-start
  0.6 0.0 copy-start.1
  0.7 0.9 copy.28
  1.6 0.1 eq.59
  1.7 0.1 eq.55
  1.9 1.2 convert_reduce_fusion
  3.1 1.3 fusion.6
  4.4 0.6 reduce-window.6
  5.0 0.2 slice_reduce_fusion
  5.3 0.1 fusion.29
  5.4 0.1 reduce_sum.41
  5.5 0.1 copy.30
  5.6 0.7 multiply_add_fusion
  6.3 0.0 copy-done.1
  6.3 2.6 %convolution_convert_fusion = bf16[384,2048]{1,0:T(8,128)(2,1)} fusion(s32[128]{0:T(128)S(1)} %get-tuple-element.11, s32[128]{0:T(128)S(1)} %get-tuple-element.10, bf16[128,2048]{1,0:T(8,128)(2,1)S(1)} %copy-done.1, f32[2048]{0:T(1024)} %param.27, f32[128]{0:T(128)S(1)} %add_rsqrt_fusion, f32[128]{0:T(128)S(1)} %broadcast_multiply_fusion), kind=kOutput, calls=%fused_computation | convolution fusion | flops 203571200 | bytes 2107392 | tf_op jit(solution)/shard_map/dot_general | solution.py:566
  8.9 0.0 copy-start.5
  8.9 0.0 copy-start.3
  8.9 5.3 %all-to-all-start = ((bf16[4,96,2048]{2,1,0:T(8,128)(2,1)}), bf16[4,96,2048]{2,1,0:T(8,128)(2,1)}, u32[]{:S(2)}, u32[]{:S(2)}) async-start(bf16[4,96,2048]{2,1,0:T(8,128)(2,1)} %bitcast.34), calls=%async_computation | async-start | bytes 3145728 | tf_op jit(solution)/shard_map/all_to_all | solution.py:570
  14.2 0.0 copy-done.5
  14.2 1.6 constant_dynamic-slice_fusion.slab_ref
  15.8 0.0 copy-done.3
  15.8 2.5 %pad_maximum_fusion.weight_ref = bf16[6,64,2048]{2,1,0:T(8,128)(2,1)} fusion(bf16[2,64,2048]{2,1,0:T(8,128)(2,1)S(1)} %bitcast.35, bf16[2,64,2048]{2,1,0:T(8,128)(2,1)} %bitcast.36, bf16[2,64,2048]{2,1,0:T(8,128)(2,1)} %bitcast.37), kind=kLoop, calls=%fused_computation.4 | loop fusion | flops 1572864 | bytes 3145728 | tf_op jit(solution)/shard_map/concatenate | solution.py:634
  18.3 124.5 %shard_map.185 = (bf16[128,1024]{1,0:T(8,128)(2,1)}, bf16[3072,2048]{1,0:T(8,128)(2,1)}, bf16[1024,2048]{1,0:T(8,128)(2,1)}) custom-call(bf16[1024,128]{1,0:T(8,128)(2,1)} %r_ref.1, bf16[1024,128]{1,0:T(8,128)(2,1)} %k_ref.1, bf16[1024,128]{1,0:T(8,128)(2,1)} %v_ref.1, bf16[1024,128]{1,0:T(8,128)(2,1)} %d_ref.1, bf16[1024,128]{1,0:T(8,128)(2,1)} %b_ref.1, ...), custom_call_target="tpu_custom_call" | custom-call | flops 6710886400 | bytes 33554432 | tf_op jit(solution)/shard_map/pallas_call | solution.py:471
  142.8 0.0 all-to-all-done
  142.8 8.1 %shard_map.187 = bf16[4,2,48,2048]{3,2,1,0:T(8,128)(2,1)} custom-call(bf16[4,2,48,2048]{3,2,1,0:T(8,128)(2,1)} %bitcast.11.x_ref, bf16[6,512,2048]{2,1,0:T(8,128)(2,1)} %bitcast.30, bf16[6,512,2048]{2,1,0:T(8,128)(2,1)} %bitcast.31, bf16[6,512,2048]{2,1,0:T(8,128)(2,1)} %bitcast.32), custom_call_target="tpu_custom_call" | custom-call | flops 2415919104 | bytes 16777216 | tf_op jit(solution)/shard_map/pallas_call | solution.py:579
  151.0 4.3 %all-to-all-start.1 = ((bf16[4,96,2048]{2,1,0:T(8,128)(2,1)}), bf16[4,96,2048]{2,1,0:T(8,128)(2,1)}, u32[]{:S(2)}, u32[]{:S(2)}) async-start(bf16[4,96,2048]{2,1,0:T(8,128)(2,1)} %bitcast.33), calls=%async_computation.1 | async-start | bytes 3145728 | tf_op jit(solution)/shard_map/all_to_all | solution.py:594
  155.3 0.0 copy-start.4
  155.3 3.5 %shard_map.186 = bf16[128,2048]{1,0:T(8,128)(2,1)} custom-call(bf16[128,1024]{1,0:T(8,128)(2,1)} %get-tuple-element.5.rows_ref, bf16[1024,2048]{1,0:T(8,128)(2,1)} %get-tuple-element.6.weight_ref), custom_call_target="tpu_custom_call" | custom-call | flops 536870912 | bytes 5242880 | tf_op jit(solution)/shard_map/pallas_call | solution.py:648
  158.8 0.0 copy-done.4
  158.8 2.1 %fusion.37 = f32[128,512]{1,0:T(8,128)S(1)} fusion(bf16[2048,512]{1,0:T(8,128)(2,1)} %param.33, bf16[128,2048]{1,0:T(8,128)(2,1)S(1)} %copy-done.1, f32[2048]{0:T(1024)S(1)} %copy-done.4, f32[128]{0:T(128)S(1)} %add_rsqrt_fusion, f32[128]{0:T(128)S(1)} %broadcast_multiply_fusion), kind=kOutput, calls=%fused_computation.54 | convolution fusion | flops 269746176 | bytes 2892800 | tf_op jit(solution)/shard_map/dot_general | solution.py:573
  160.9 0.0 copy-done
  160.9 3.5 %fusion.5 = f32[128,2048]{1,0:T(8,128)} fusion(bf16[512,2048]{1,0:T(8,128)(2,1)S(1)} %copy-done, bf16[2048,512]{1,0:T(8,128)(2,1)} %param.34, f32[128,512]{1,0:T(8,128)S(1)} %fusion.37, bf16[128,2048]{1,0:T(8,128)(2,1)S(1)} %copy-done.1, f32[2048]{0:T(1024)S(1)} %copy-done.4, f32[128]{0:T(128)S(1)} %add_rsqrt_fusion, f32[128]{0:T(128)S(1)} %broadcast_multiply_fusion), kind=kOutput, calls=%fused_computation.11 | convolution fusion | flops 538574848 | bytes 6038528 | tf_op jit(solution)/shard_map/dot_general | solution.py:576
  164.4 11.1 %all-to-all-done.1 = bf16[4,96,2048]{2,1,0:T(8,128)(2,1)} async-done(((bf16[4,96,2048]{2,1,0:T(8,128)(2,1)}), bf16[4,96,2048]{2,1,0:T(8,128)(2,1)}, u32[]{:S(2)}, u32[]{:S(2)}) %all-to-all-start.1) | async-done | bytes 1572896 | tf_op jit(solution)/shard_map/all_to_all | solution.py:594
  175.5 0.0 copy-start.2
  175.5 2.0 %fusion.26 = f32[128,2048]{1,0:T(8,128)S(1)} fusion(bf16[384,2048]{1,0:T(8,128)(2,1)} %bitcast.14, f32[128]{0:T(128)S(1)} %get-tuple-element.9, s32[128]{0:T(128)S(1)} %get-tuple-element.11, f32[128]{0:T(128)S(1)} %get-tuple-element.8, s32[128]{0:T(128)S(1)} %get-tuple-element.10), kind=kOutput, calls=%fused_computation.34 | convolution fusion | flops 201621504 | bytes 2623488 | tf_op jit(solution)/shard_map/dot_general | solution.py:601
  177.5 0.0 copy-done.2
  177.5 2.7 %fusion.1 = bf16[128,2048]{1,0:T(8,128)(2,1)} fusion(f32[128,2048]{1,0:T(8,128)S(1)} %copy-done.2, f32[128,2048]{1,0:T(8,128)S(1)} %fusion.26, bf16[384,2048]{1,0:T(8,128)(2,1)} %bitcast.14, f32[128]{0:T(128)S(1)} %get-tuple-element.9, s32[128]{0:T(128)S(1)} %get-tuple-element.11, f32[128]{0:T(128)S(1)} %get-tuple-element.8, s32[128]{0:T(128)S(1)} %get-tuple-element.10), kind=kOutput, calls=%fused_computation.3 | convolution fusion | flops 202555392 | bytes 4196352 | tf_op jit(solution)/shard_map/dot_general | solution.py:601
  (9 shorter events, 0.1 us)
Async XLA Ops:
  0.6 160.3 %copy-start = (bf16[512,2048]{1,0:T(8,128)(2,1)S(1)}, bf16[512,2048]{1,0:T(8,128)(2,1)}, u32[]{:S(2)}) copy-start(bf16[512,2048]{1,0:T(8,128)(2,1)} %param.35) | copy-start | bytes 6291460
  0.6 5.7 %copy-start.1 = (bf16[128,2048]{1,0:T(8,128)(2,1)S(1)}, bf16[128,2048]{1,0:T(8,128)(2,1)}, u32[]{:S(2)}) copy-start(bf16[128,2048]{1,0:T(8,128)(2,1)} %param.26) | copy-start | bytes 1572868
  8.9 5.3 %copy-start.5 = (f32[128,2]{0,1:T(2,128)S(1)}, f32[128,2]{0,1:T(2,128)}, u32[]{:S(2)}) copy-start(f32[128,2]{0,1:T(2,128)} %param.29) | copy-start | bytes 3076
  8.9 6.9 %copy-start.3 = (bf16[2,2048,64]{1,2,0:T(8,128)(2,1)S(1)}, bf16[2,2048,64]{1,2,0:T(8,128)(2,1)}, u32[]{:S(2)}) copy-start(bf16[2,2048,64]{1,2,0:T(8,128)(2,1)} %param.32) | copy-start | bytes 1572868
  8.9 134.0 %all-to-all-start = ((bf16[4,96,2048]{2,1,0:T(8,128)(2,1)}), bf16[4,96,2048]{2,1,0:T(8,128)(2,1)}, u32[]{:S(2)}, u32[]{:S(2)}) async-start(bf16[4,96,2048]{2,1,0:T(8,128)(2,1)} %bitcast.34), calls=%async_computation | async-start | bytes 3145728 | tf_op jit(solution)/shard_map/all_to_all | solution.py:570
  151.0 24.5 %all-to-all-start.1 = ((bf16[4,96,2048]{2,1,0:T(8,128)(2,1)}), bf16[4,96,2048]{2,1,0:T(8,128)(2,1)}, u32[]{:S(2)}, u32[]{:S(2)}) async-start(bf16[4,96,2048]{2,1,0:T(8,128)(2,1)} %bitcast.33), calls=%async_computation.1 | async-start | bytes 3145728 | tf_op jit(solution)/shard_map/all_to_all | solution.py:594
  155.3 3.5 %copy-start.4 = (f32[2048]{0:T(1024)S(1)}, f32[2048]{0:T(1024)}, u32[]{:S(2)}) copy-start(f32[2048]{0:T(1024)} %param.27) | copy-start | bytes 24580
  175.5 2.0 %copy-start.2 = (f32[128,2048]{1,0:T(8,128)S(1)}, f32[128,2048]{1,0:T(8,128)}, u32[]{:S(2)}) copy-start(f32[128,2048]{1,0:T(8,128)} %fusion.5) | copy-start | bytes 3145732
where the time goes:
time: 181 us; the launch traced here: 180 us
  Pallas kernels  136 us (75%)
  matrix products  12.8 us (7%)
  waiting for transfers between devices  11.1 us (6%)
  starting transfers between devices  9.66 us (5%)
  other arithmetic  6.5 us (4%)
  local copies, waits for them, and re-layouts  3.25 us (2%)
    pallas_call x1, Pallas kernels, mixer_and_weights(): pl.pallas_call(functools.partial(mixer_kernel, 4, groups, ring), out_shap...  125 us
    all_to_all x1, waiting for transfers between devices, expert_layer(): lax.all_to_all(sending, 'ep', split_axis=0, concat_axis=0, tiled=True)  11.1 us
    pallas_call x1, Pallas kernels, expert_layer(): pl.pallas_call(ffn_kernel, grid=(local_count,), out_shape=jax.ShapeDtypeS...  8.14 us
    all_to_all x1, starting transfers between devices, expert_layer(): lax.all_to_all(outgoing, 'ep', split_axis=0, concat_axis=0, tiled=True)  5.32 us
    all_to_all x1, starting transfers between devices, expert_layer(): lax.all_to_all(sending, 'ep', split_axis=0, concat_axis=0, tiled=True)  4.34 us
  transfers between devices with their start and end apart: 2, of which 1 were waited for; matrix products, arithmetic and copies ran while one was open for 5% of the time, Pallas kernels for 71%

commit v1 on v0

v1 whole, which is shorter than its diff:
```python
import functools

import jax
import jax.numpy as jnp
from jax import lax
from jax.experimental import pallas as pl
from jax.experimental.pallas import tpu as pltpu
from jax.sharding import PartitionSpec as P

HEAD_DIM = 64
BLOCK = 64


def dims(form):
    return {"nn": ((1,), (0,)), "nt": ((1,), (1,)), "tn": ((0,), (0,))}[form]


def mm1(left, right, form="nn"):
    return lax.dot_general(
        left.astype(jnp.bfloat16),
        right.astype(jnp.bfloat16),
        (dims(form), ((), ())),
        preferred_element_type=jnp.float32,
    )


def mm3(left, right, form="nn"):
    lh, rh = left.astype(jnp.bfloat16), right.astype(jnp.bfloat16)
    ll = (left - lh.astype(jnp.float32)).astype(jnp.bfloat16)
    rl = (right - rh.astype(jnp.float32)).astype(jnp.bfloat16)
    return mm1(lh, rh, form) + (mm1(lh, rl, form) + mm1(ll, rh, form))


mm_g = mm3
mm_inv = mm3
mm_q = mm3
mm_out = mm3
mm_car = mm3
mm_scan = mm3


def head_masks(rows, width):
    lane = lax.broadcasted_iota(jnp.int32, (rows, width), 1)
    return lane < HEAD_DIM


def stacked(x):
    first = head_masks(*x.shape)
    return jnp.concatenate([jnp.where(first, x, 0.0), jnp.where(first, 0.0, x)], axis=0)


def per_head_sum(x):
    first = head_masks(*x.shape)
    one = jnp.sum(jnp.where(first, x, 0.0), axis=-1, keepdims=True)
    both = jnp.sum(jnp.where(first, 0.0, x), axis=-1, keepdims=True)
    return jnp.where(first, one, both)


def sigmoid(x):
    return 1.0 / (1.0 + jnp.exp(-x))


def local_block(r_in, k_in, v_in, d_in, b_in):
    f32 = jnp.float32
    keys = k_in.astype(f32)
    unit = keys * lax.rsqrt(per_head_sum(keys * keys) + 1e-06)
    log_decay = sigmoid(d_in.astype(f32)) * -0.6065306597126334
    tri_row = lax.broadcasted_iota(jnp.int32, (BLOCK, 3 * BLOCK), 0)
    tri_col = lax.broadcasted_iota(jnp.int32, (BLOCK, 3 * BLOCK), 1) % BLOCK
    tri = jnp.where(tri_col <= tri_row, 1.0, 0.0).astype(jnp.bfloat16)
    hi = log_decay.astype(jnp.bfloat16)
    rest = log_decay - hi.astype(f32)
    mid = rest.astype(jnp.bfloat16)
    low = (rest - mid.astype(f32)).astype(jnp.bfloat16)
    cumul = mm1(tri, jnp.concatenate([hi, mid, low], axis=0))
    end_scale = jnp.exp(cumul[BLOCK - 1 :, :])
    shrink = jnp.exp(-cumul)
    query2 = stacked(r_in.astype(f32) * jnp.exp(cumul))
    alpha2 = stacked(-unit * jnp.exp(cumul - log_decay))
    key_grow = keys * shrink
    beta_grow = unit * sigmoid(b_in.astype(f32)) * shrink
    values2 = stacked(v_in.astype(f32))
    two = 2 * BLOCK
    grams = mm_g(
        jnp.concatenate([alpha2, query2], axis=0),
        jnp.concatenate([beta_grow, beta_grow, key_grow, key_grow], axis=0),
        "nt",
    )
    row = lax.broadcasted_iota(jnp.int32, (two, two), 0)
    col = lax.broadcasted_iota(jnp.int32, (two, two), 1)
    same = row // BLOCK == col // BLOCK
    strict = same & (col < row)
    inclusive = same & (col <= row)
    couple = jnp.where(strict, grams[:two, :two], 0.0)
    insert = jnp.where(strict, grams[:two, two:], 0.0)
    read_beta = jnp.where(inclusive, grams[two:, :two], 0.0)
    read_key = jnp.where(inclusive, grams[two:, two:], 0.0)
    size = 8
    near = jnp.where(row // size == col // size, couple, 0.0)
    inverse = jnp.where(row == col, 1.0, 0.0) + near
    power = mm_inv(near, near)
    both = mm_inv(jnp.concatenate([inverse, power], axis=0), power)
    inverse = inverse + both[:two]
    inverse = inverse + mm_inv(inverse, both[two:])
    while size < BLOCK:
        wide = 2 * size
        off = jnp.where(
            (row // wide == col // wide) & (row // size != col // size), couple, 0.0
        )
        inverse = inverse + mm_inv(inverse, mm_inv(off, inverse))
        size = wide
    inserted = mm_q(insert, values2)
    qz = mm_q(inverse, jnp.concatenate([alpha2, inserted], axis=1))
    lower = jnp.concatenate([jnp.zeros_like(values2), values2], axis=1)
    stack = jnp.concatenate([qz, lower], axis=0)
    reads = mm_out(jnp.concatenate([read_beta, read_key], axis=1), stack)
    query_bar = query2 + reads[:, :two]
    local_out = reads[:, two:]
    ends = jnp.concatenate([stacked(beta_grow * end_scale), stacked(key_grow * end_scale)], axis=0)
    maps = mm_car(stack, ends, "tn")
    return query_bar, local_out, maps, end_scale


def silu(x):
    return x / (1.0 + jnp.exp(-x))


def layer_kernel(
    unroll,
    pieces,
    slots,
    r_ref,
    k_ref,
    v_ref,
    d_ref,
    b_ref,
    gate_ref,
    gain_ref,
    x_ref,
    moe_gain_ref,
    routes_ref,
    scores_ref,
    project_in,
    expert_gate,
    expert_up,
    expert_down,
    shared_gate,
    shared_up,
    shared_down,
    mixed_ref,
    moe_ref,
    state,
    qp_ref,
    lo_ref,
    rows_ref,
    totals,
    token_ref,
    project,
    weights,
    shared_one,
    shared_two,
    shared_three,
    shared_hidden,
    shared_term,
    others,
    other_routes,
    other_scores,
    normal,
    chosen_ref,
    spread_ref,
    leaving,
    arrived,
    returned,
    hidden_ref,
    part_out,
    part_in,
    token_send,
    token_recv,
    slab_send,
    slab_recv,
    wide_send,
    wide_recv,
    pair_send,
    pair_recv,
    core_send,
    core_recv,
    relay_send,
    relay_recv,
    load_sem,
    go_send,
    go_recv,
    back_send,
    back_recv,
    part_send,
    part_recv,
    ep_send,
    ep_recv,
    row_send,
    row_recv,
):
    f32, bf16 = jnp.float32, jnp.bfloat16
    two = 2 * BLOCK
    MESH = pl.DeviceIdType.MESH
    here, mine = lax.axis_index("ep"), lax.axis_index("tp")
    groups, peers = lax.axis_size("ep"), lax.axis_size("tp")
    depth, core = mine // 2, mine % 2
    teams = peers // 4
    team, side = depth // 2, depth % 2
    seat = side * 2 + core
    facing = (1 - side) * 2 + core
    partner = depth * 2 + 1 - core
    across = team * 4 + facing
    tokens, width = x_ref.shape
    local, height = expert_gate.shape[0], expert_gate.shape[1]
    experts = local * groups
    span = local * slots
    columns = width // groups
    piece = width // pieces
    sources = (expert_gate, expert_up, expert_down)
    kinds = len(sources)

    def remote(source, target, send, recv, device):
        return pltpu.make_async_remote_copy(
            src_ref=source,
            dst_ref=target,
            send_sem=send,
            recv_sem=recv,
            device_id=device,
            device_id_type=MESH,
        )

    def mate(shift):
        return {"tp": (team + shift) % teams * 4 + seat}

    def column(shift):
        return {"ep": (here + groups + shift) % groups}

    def token_copies(s):
        pairs = ((x_ref, others), (routes_ref, other_routes), (scores_ref, other_scores))
        return [
            remote(a, b.at[s], token_send.at[s, i], token_recv.at[s, i], mate(s))
            for i, (a, b) in enumerate(pairs)
        ]

    def slab_place(owner, part):
        return project.at[
            pl.ds(pl.multiple_of(owner * two, two), two),
            pl.ds(pl.multiple_of(part * columns, columns), columns),
        ]

    def slab_copy(s):
        source = project_in.at[:, pl.ds(pl.multiple_of(here * columns, columns), columns)]
        return remote(
            source, slab_place(mine, here), slab_send.at[s], slab_recv.at[s], mate(s)
        )

    def wide_copy(s, q):
        owner = (team + teams - s) % teams * 4 + seat
        block = slab_place(owner, here)
        return remote(block, block, wide_send.at[s, q], wide_recv.at[s, q], column(q))

    def weight_place(a, owner):
        if a < kinds:
            return weights.at[
                pl.ds(a * local, local), pl.ds(pl.multiple_of(owner * height, height), height), :
            ]
        return project_place(0, owner)

    def project_place(s, owner):
        base = (team + teams - s) % teams * 4 + owner
        return project.at[pl.ds(pl.multiple_of(base * two, two), two), :]

    def place_of(a, owner):
        return weight_place(a, owner) if a <= kinds else project_place(a - kinds, owner)

    def own_block(a):
        if a < kinds:
            return sources[a]
        return project_in if a == kinds else project_place(a - kinds, seat)

    def pair_copy(a):
        return remote(
            own_block(a), place_of(a, seat), pair_send.at[a], pair_recv.at[a], {"tp": across}
        )

    def core_copy(a):
        return remote(
            own_block(a), place_of(a, seat), core_send.at[a], core_recv.at[a], {"tp": partner}
        )

    def relay_copy(a):
        block = place_of(a, facing)
        return remote(block, block, relay_send.at[a], relay_recv.at[a], {"tp": partner})

    def own_copy(a):
        return pltpu.make_async_copy(own_block(a), place_of(a, seat), load_sem.at[a])

    def relay(a):
        pair_copy(a).wait_recv()
        relay_copy(a).start()

    def ready(a):
        core_copy(a).wait_recv()
        relay_copy(a).wait_recv()

    def shared_copy(i):
        source = (shared_gate, shared_up, shared_down)[i]
        target = (shared_one, shared_two, shared_three)[i]
        return pltpu.make_async_copy(source, target, load_sem.at[kinds + 1 + i])

    def go_copy(s, q):
        return remote(
            leaving.at[s, q], arrived.at[s, q], go_send.at[s, q], go_recv.at[s, q], column(q)
        )

    def back_copy(s, q, n):
        cols = pl.ds(pl.multiple_of(n * piece, piece), piece)
        return remote(
            arrived.at[s, q, :, cols],
            returned.at[s, q, :, cols],
            back_send.at[s, q, n],
            back_recv.at[s, q, n],
            column(-q),
        )

    def part_copy(s, n):
        cols = pl.ds(pl.multiple_of(n * piece, piece), piece)
        return remote(
            part_out.at[s, :, cols],
            part_in.at[s, :, cols],
            part_send.at[s, n],
            part_recv.at[s, n],
            mate(teams - s),
        )

    barrier = pltpu.get_barrier_semaphore()
    for q in range(1, peers):
        pl.semaphore_signal(
            barrier, inc=1, device_id={"tp": (mine + q) % peers}, device_id_type=MESH
        )
    for q in range(1, groups):
        pl.semaphore_signal(
            barrier, inc=1, device_id={"ep": (here + q) % groups}, device_id_type=MESH
        )
    pl.semaphore_wait(barrier, peers + groups - 2)

    for s in range(1, teams):
        for copy in token_copies(s):
            copy.start()
    for a in range(kinds + 1):
        pair_copy(a).start()
        core_copy(a).start()
        own_copy(a).start()
    for s in range(1, teams):
        slab_copy(s).start()
    for i in range(3):
        shared_copy(i).start()

    def normalize(source, target):
        tall = 16

        def some(i, carry):
            rows = pl.ds(pl.multiple_of(i * tall, tall), tall)
            values = source[rows, :].astype(f32)
            centered = values - jnp.sum(values, -1, keepdims=True) * (1.0 / width)
            spread = jnp.sum(centered * centered, -1, keepdims=True) * (1.0 / width)
            target[rows, :] = (centered * lax.rsqrt(spread + 1e-05) * moe_gain_ref[...]).astype(
                bf16
            )
            return carry

        lax.fori_loop(0, tokens // tall, some, 0)

    def dispatch(s, source, routes, scores, held):
        normalize(source, normal.at[held])
        count = max(16, experts)
        order = lax.broadcasted_iota(jnp.int32, (count, tokens), 0)
        names = (here + order // local) % groups * local + order % local
        names = jnp.where(order < experts, names, -1)
        tops = routes.shape[0]
        hits = [routes[k : k + 1, :] == names for k in range(tops)]
        picks = sum(jnp.where(hit, 1.0, 0.0) for hit in hits)
        past = lax.broadcasted_iota(jnp.int32, (tokens, tokens), 0)
        present = lax.broadcasted_iota(jnp.int32, (tokens, tokens), 1)
        earlier = mm1(picks, jnp.where(past < present, 1.0, 0.0))
        index = order.astype(f32) * slots + earlier
        row = lax.broadcasted_iota(jnp.int32, (experts * slots, tokens), 0).astype(f32)
        match = [
            row == jnp.sum(jnp.where(hit, index, 0.0), axis=0, keepdims=True) for hit in hits
        ]
        total = sum(scores[k : k + 1, :] for k in range(tops))
        chosen_ref[...] = sum(jnp.where(m, 1.0, 0.0) for m in match).astype(bf16)
        spread = sum(
            jnp.where(match[k], 2.5 * scores[k : k + 1, :] / total, 0.0) for k in range(tops)
        )
        spread_ref[s] = jnp.transpose(spread).astype(bf16)
        step = 256

        def fill(i, carry):
            cols = pl.ds(pl.multiple_of(i * step, step), step)
            out = jnp.dot(
                chosen_ref[...], normal[held, :, cols], preferred_element_type=f32
            ).astype(bf16)
            arrived[s, 0, :, cols] = out[:span]
            leaving[s, 1:, :, cols] = out[span:].reshape(groups - 1, span, step)
            return carry

        lax.fori_loop(0, width // step, fill, 0)

        def send(q, carry):
            go_copy(s, q).start()
            return carry

        lax.fori_loop(1, groups, send, 0)

    dispatch(0, x_ref, routes_ref, scores_ref, 0)

    row = lax.broadcasted_iota(jnp.int32, (2 * two, two), 0)
    col = lax.broadcasted_iota(jnp.int32, (2 * two, two), 1)
    state[...] = jnp.where(row == col, 1.0, 0.0)
    turns = r_ref.shape[0] // (BLOCK * unroll)

    def turn(step, carry):
        parts = []
        for u in range(unroll):
            rows = pl.ds(pl.multiple_of((step * unroll + u) * BLOCK, BLOCK), BLOCK)
            parts.append(
                local_block(
                    r_ref[rows, :], k_ref[rows, :], v_ref[rows, :], d_ref[rows, :], b_ref[rows, :]
                )
            )
        now = state[...]
        for u, (query_bar, local_out, maps, end_scale) in enumerate(parts):
            rows = pl.ds(pl.multiple_of((step * unroll + u) * BLOCK, BLOCK), BLOCK)
            out = mm_scan(query_bar, now, "nt")
            qp_ref[rows, :] = out[:BLOCK, :two] + out[BLOCK:, :two]
            lo = out[:, two:] + local_out
            lo_ref[rows, :] = lo[:BLOCK] + lo[BLOCK:]
            moved = mm_scan(now, maps[:two]) + now * end_scale
            now = jnp.concatenate([moved[:two], moved[two:] + maps[two:]], axis=0)
        state[...] = now
        return carry

    lax.fori_loop(0, turns, turn, 0)

    carry_map, source_map = state[:two, :], state[two:, :]
    totals[here, 0] = (carry_map[:BLOCK] + carry_map[BLOCK:]).astype(totals.dtype)
    totals[here, 1] = (source_map[:BLOCK] + source_map[BLOCK:]).astype(totals.dtype)

    def ep_copy(q, slot):
        return remote(
            totals.at[slot], totals.at[slot], ep_send.at[q], ep_recv.at[q], column(q)
        )

    for q in range(1, groups):
        ep_copy(q, here).start()

    relay(0)

    def receive(s, carry):
        for copy in token_copies(s):
            copy.wait_recv()
        dispatch(s, others.at[s], other_routes.at[s], other_scores.at[s], 1)
        slab_copy(s).wait_recv()

        def widen(q, inner):
            wide_copy(s, q).start()
            return inner

        lax.fori_loop(1, groups, widen, 0)
        return carry

    lax.fori_loop(1, teams, receive, 0)

    for i in range(3):
        shared_copy(i).wait()
    step = 256
    for i in range(shared_one.shape[1] // step):
        cols = slice(i * step, (i + 1) * step)
        gate = jnp.dot(normal[0], shared_one[:, cols], preferred_element_type=f32)
        upper = jnp.dot(normal[0], shared_two[:, cols], preferred_element_type=f32)
        shared_hidden[:, cols] = (silu(gate) * upper).astype(bf16)

    def share(i, carry):
        cols = pl.ds(pl.multiple_of(i * step, step), step)
        shared_term[:, cols] = jnp.dot(
            shared_hidden[...], shared_three[:, cols], preferred_element_type=f32
        )
        return carry

    lax.fori_loop(0, width // step, share, 0)

    for q in range(1, groups):
        ep_copy(q, (here + groups - q) % groups).wait_recv()

    def enter(k, entry):
        carry = stacked(totals[k, 0].astype(f32))
        source = stacked(totals[k, 1].astype(f32))
        reached = jnp.where(k < here, 1.0, 0.0)
        return entry + reached * (mm3(entry, carry) + source - entry)

    entry = lax.fori_loop(0, groups, enter, jnp.zeros((two, two), f32))

    def row_copy(q, target, source):
        return remote(
            rows_ref.at[pl.ds(pl.multiple_of(target * tokens, tokens), tokens), :],
            token_ref.at[:, pl.ds(pl.multiple_of(source * two, two), two)],
            row_send.at[q],
            row_recv.at[q],
            {"tp": target},
        )

    def finish(rows):
        recur = mm3(qp_ref[rows, :], entry, "nt") + lo_ref[rows, :]
        centered = recur - per_head_sum(recur) * (1.0 / HEAD_DIM)
        spread = per_head_sum(centered * centered) * (1.0 / HEAD_DIM)
        normed = centered * lax.rsqrt(spread + 0.00064)
        gated = normed * gain_ref[...] * sigmoid(gate_ref[rows, :].astype(f32))
        rows_ref[rows, :] = gated.astype(bf16)

    def finish_turn(q, carry):
        finish(pl.ds(pl.multiple_of(q * tokens, tokens), tokens))
        return carry

    lax.fori_loop(0, peers, finish_turn, 0)
    own_rows = pltpu.make_async_copy(
        rows_ref.at[pl.ds(pl.multiple_of(mine * tokens, tokens), tokens), :],
        token_ref.at[:, pl.ds(pl.multiple_of(mine * two, two), two)],
        load_sem.at[kinds + 4],
    )
    own_rows.start()

    def row_start(q, carry):
        row_copy(q, (mine + q) % peers, mine).start()
        return carry

    lax.fori_loop(1, peers, row_start, 0)

    for a in range(1, kinds):
        relay(a)
    for a in range(kinds):
        own_copy(a).wait()
        ready(a)
    nt = (((1,), (1,)), ((), ()))

    def feed(i, carry):
        s = (i + 1) % teams

        def come(q, inner):
            go_copy(s, q).wait_recv()
            return inner

        lax.fori_loop(1, groups, come, 0)
        for e in range(local):
            mine_slots = slice(e * slots, (e + 1) * slots)
            x = arrived[s, :, mine_slots, :].reshape(groups * slots, width)
            gate = lax.dot_general(x, weights[e], nt, preferred_element_type=f32)
            upper = lax.dot_general(x, weights[local + e], nt, preferred_element_type=f32)
            hidden_ref[e] = (silu(gate) * upper).astype(bf16)

        def down(n, inner):
            cols = pl.ds(pl.multiple_of(n * piece, piece), piece)
            for e in range(local):
                mine_slots = slice(e * slots, (e + 1) * slots)
                out = jnp.dot(
                    hidden_ref[e], weights[2 * local + e, :, cols], preferred_element_type=f32
                )
                out = out.astype(bf16).reshape(groups, slots, piece)
                returned[s, 0, mine_slots, cols] = out[0]
                arrived[s, 1:, mine_slots, cols] = out[1:]

            def back(q, last):
                back_copy(s, q, n).start()
                return last

            return lax.fori_loop(1, groups, back, inner)

        return lax.fori_loop(0, pieces, down, carry)

    lax.fori_loop(0, teams, feed, 0)

    relay(kinds)
    for s in range(1, teams):

        def widened(q, carry, s=s):
            wide_copy(s, q).wait_recv()
            return carry

        lax.fori_loop(1, groups, widened, 0)
        pair_copy(kinds + s).start()
        core_copy(kinds + s).start()

    def combined(s, n):
        def come(q, carry):
            back_copy(s, q, n).wait_recv()
            return carry

        lax.fori_loop(1, groups, come, 0)
        cols = pl.ds(pl.multiple_of(n * piece, piece), piece)
        rows = returned[s, :, :, cols].reshape(groups * span, piece)
        return jnp.dot(spread_ref[s], rows, preferred_element_type=f32), cols

    def partial(s, carry):
        def some(n, inner):
            value, cols = combined(s, n)
            part_out[s, :, cols] = value.astype(bf16)
            part_copy(s, n).start()
            return inner

        return lax.fori_loop(0, pieces, some, carry)

    lax.fori_loop(1, teams, partial, 0)

    for a in range(kinds + 1, kinds + teams):
        relay(a)
    own_copy(kinds).wait()
    for a in range(kinds, kinds + teams):
        ready(a)
    own_rows.wait()

    def row_end(q, carry):
        row_copy(q, (mine + q) % peers, (mine + peers - q) % peers).wait()
        return carry

    lax.fori_loop(1, peers, row_end, 0)

    def mix(i, carry):
        cols = pl.ds(pl.multiple_of(i * step, step), step)
        mixed_ref[:, cols] = jnp.dot(
            token_ref[...], project[:, cols], preferred_element_type=f32
        ).astype(bf16)
        return carry

    lax.fori_loop(0, width // step, mix, 0)

    def close(n, carry):
        value, cols = combined(0, n)
        total = value + shared_term[:, cols]
        for s in range(1, teams):
            part_copy(s, n).wait_recv()
            total = total + part_in[s, :, cols].astype(f32)
        moe_ref[:, cols] = total.astype(bf16)
        return carry

    lax.fori_loop(0, pieces, close, 0)

    for a in range(kinds + teams):
        pair_copy(a).wait_send()
        core_copy(a).wait_send()
        relay_copy(a).wait_send()
    for q in range(1, groups):
        ep_copy(q, here).wait_send()

    def sent(s, carry):
        def each(q, inner):
            go_copy(s, q).wait_send()

            def block(n, last):
                back_copy(s, q, n).wait_send()
                return last

            return lax.fori_loop(0, pieces, block, inner)

        return lax.fori_loop(1, groups, each, carry)

    lax.fori_loop(0, teams, sent, 0)

    def shipped(s, carry):
        for copy in token_copies(s):
            copy.wait_send()
        slab_copy(s).wait_send()

        def each(q, inner):
            wide_copy(s, q).wait_send()
            return inner

        def block(n, inner):
            part_copy(s, n).wait_send()
            return inner

        lax.fori_loop(1, groups, each, 0)
        return lax.fori_loop(0, pieces, block, carry)

    lax.fori_loop(1, teams, shipped, 0)


def shards(
    receptance,
    key_in,
    payload_vectors,
    decay_in,
    rate_in,
    gate_in,
    norm_gain,
    out_weight,
    moe_in,
    moe_gain,
    routes,
    route_weights,
    expert_gate,
    expert_up,
    expert_down,
    shared_gate,
    shared_up,
    shared_down,
):
    length, channels = receptance.shape
    tokens, width = moe_in.shape
    groups, peers = lax.axis_size("ep"), lax.axis_size("tp")
    teams = peers // 4
    local, _, height = expert_gate.shape
    top_count = routes.shape[1]
    experts = local * groups
    slots = max(2, 3 * tokens * top_count // (2 * experts))
    slots = -(-slots // 16) * 16
    span = local * slots
    inner = shared_gate.shape[1]
    pieces = 4
    kinds = 3
    wide = 2 * HEAD_DIM
    spare = wide - channels
    pad = lambda x: jnp.pad(x, ((0, 0),) * (x.ndim - 1) + ((0, spare),)) if spare else x
    weight_rows = jnp.pad(out_weight, ((0, spare), (0, 0))) if spare else out_weight
    f32, bf16 = jnp.float32, jnp.bfloat16
    vmem = pl.BlockSpec(memory_space=pltpu.VMEM)
    anywhere = pl.BlockSpec(memory_space=pl.ANY)
    dma = pltpu.SemaphoreType.DMA
    out = jax.ShapeDtypeStruct((tokens, width), bf16)
    turned = lambda w: jnp.swapaxes(w, 1, 2)
    return pl.pallas_call(
        functools.partial(layer_kernel, 4, pieces, slots),
        out_shape=(out, out),
        in_specs=[vmem] * 11 + [anywhere] * 7,
        out_specs=(vmem, vmem),
        scratch_shapes=[
            pltpu.VMEM((2 * wide, wide), f32),
            pltpu.VMEM((length, wide), f32),
            pltpu.VMEM((length, wide), f32),
            pltpu.VMEM((length, wide), bf16),
            pltpu.VMEM((groups, 2, HEAD_DIM, wide), bf16),
            pltpu.VMEM((tokens, peers * wide), bf16),
            pltpu.VMEM((peers * wide, width), bf16),
            pltpu.VMEM((kinds * local, 4 * height, width), bf16),
            pltpu.VMEM(shared_gate.shape, bf16),
            pltpu.VMEM(shared_up.shape, bf16),
            pltpu.VMEM(shared_down.shape, bf16),
            pltpu.VMEM((tokens, inner), bf16),
            pltpu.VMEM((tokens, width), f32),
            pltpu.VMEM((teams, tokens, width), bf16),
            pltpu.VMEM((teams, top_count, tokens), jnp.int32),
            pltpu.VMEM((teams, top_count, tokens), f32),
            pltpu.VMEM((2, tokens, width), bf16),
            pltpu.VMEM((experts * slots, tokens), bf16),
            pltpu.VMEM((teams, tokens, experts * slots), bf16),
            pltpu.VMEM((teams, groups, span, width), bf16),
            pltpu.VMEM((teams, groups, span, width), bf16),
            pltpu.VMEM((teams, groups, span, width), bf16),
            pltpu.VMEM((local, groups * slots, 4 * height), bf16),
            pltpu.VMEM((teams, tokens, width), bf16),
            pltpu.VMEM((teams, tokens, width), bf16),
            dma((teams, 3)),
            dma((teams, 3)),
            dma((teams,)),
            dma((teams,)),
            dma((teams, groups)),
            dma((teams, groups)),
            dma((kinds + teams,)),
            dma((kinds + teams,)),
            dma((kinds + teams,)),
            dma((kinds + teams,)),
            dma((kinds + teams,)),
            dma((kinds + teams,)),
            dma((kinds + 5,)),
            dma((teams, groups)),
            dma((teams, groups)),
            dma((teams, groups, pieces)),
            dma((teams, groups, pieces)),
            dma((teams, pieces)),
            dma((teams, pieces)),
            dma((groups,)),
            dma((groups,)),
            dma((peers,)),
            dma((peers,)),
        ],
        compiler_params=pltpu.CompilerParams(
            collective_id=0, has_side_effects=True, vmem_limit_bytes=63 << 20
        ),
    )(
        pad(receptance),
        pad(key_in),
        pad(payload_vectors),
        pad(decay_in),
        pad(rate_in),
        pad(gate_in),
        pad(norm_gain).reshape(1, wide),
        moe_in,
        moe_gain.reshape(1, width),
        routes.T,
        route_weights.T,
        weight_rows,
        turned(expert_gate),
        turned(expert_up),
        turned(expert_down),
        shared_gate,
        shared_up,
        shared_down,
    )


def solution(mesh):
    placed = (
        P("ep", "tp"),
        P("ep", "tp"),
        P("ep", "tp"),
        P("ep", "tp"),
        P("ep", "tp"),
        P("ep", "tp"),
        P("tp"),
        P("tp", None),
        P(("ep", "tp"), None),
        P(),
        P(("ep", "tp"), None),
        P(("ep", "tp"), None),
        P("ep", None, "tp"),
        P("ep", None, "tp"),
        P("ep", None, "tp"),
        P(),
        P(),
        P(),
    )
    return jax.shard_map(
        shards,
        mesh=mesh,
        in_specs=placed,
        out_specs=(P(("ep", "tp"), None), P(("ep", "tp"), None)),
        check_vma=False,
    )
```

time: 181 us -> 124 us (0.69)
  Pallas kernels: 136 us -> 120 us
  matrix products: 12.8 us -> 0 us
  waiting for transfers between devices: 11.1 us -> 0 us
  starting transfers between devices: 9.66 us -> 0 us
  other arithmetic: 6.5 us -> 0 us
    pallas_call x3 -> x1, Pallas kernels: 136 us -> 120 us  [shards(): pl.pallas_call(functools.partial(layer_kernel, 4, pieces, slots), out_sha...]
    dot_general x5 -> x0, matrix products: 12.8 us -> none  [the longest x1 3.47 us: expert_layer(): jnp.dot(shared_hidden, shared_down, preferred_element_type=jnp.float32)]
    all_to_all x2 -> x0, waiting for transfers between devices: 11.1 us -> none  [the longest x1 11.1 us: expert_layer(): lax.all_to_all(sending, 'ep', split_axis=0, concat_axis=0, tiled=True)]
    all_to_all x2 -> x0, starting transfers between devices: 9.66 us -> none  [the longest x1 5.32 us: expert_layer(): lax.all_to_all(outgoing, 'ep', split_axis=0, concat_axis=0, tiled=True)]
    unnamed x13 -> x2, local copies, waits for them, and re-layouts: 0.98 us -> 3.76 us
    reduce_sum x4 -> x0, other arithmetic: 2.64 us -> none  [the longest x1 1.33 us: expert_layer(): jnp.mean(centered * centered, -1, keepdims=True) + 1e-05]
    concatenate x1 -> x0, other arithmetic: 2.51 us -> none  [shards(): jnp.concatenate([jnp.swapaxes(w, 1, 2) for w in (expert_gate, expert_up,...]
  transfers between devices with their start and end apart: 2 -> 0, of which waited for: 1 -> 0; matrix products, arithmetic and copies ran while one was open for 5% -> 0% of each run, Pallas kernels for 71% -> 0%
where the time goes in v1:
time: 124 us
  Pallas kernels  120 us (97%)
  local copies, waits for them, and re-layouts  3.76 us (3%)
    pallas_call x1, Pallas kernels, shards(): pl.pallas_call(functools.partial(layer_kernel, 4, pieces, slots), out_sha...  120 us
    unnamed x2, local copies, waits for them, and re-layouts  3.76 us

profile of v1, /device:TPU:0, one launch (start us, length us, event | category | flops | bytes accessed | tf_op | source)
XLA Modules:
  0.0 124.0 jit_solution(907236324480388242)
XLA Ops:
  0.6 119.6 %shard_map.185 = (bf16[128,2048]{1,0:T(8,128)(2,1)}, bf16[128,2048]{1,0:T(8,128)(2,1)}) custom-call(bf16[1024,128]{1,0:T(8,128)(2,1)} %r_ref.1, bf16[1024,128]{1,0:T(8,128)(2,1)} %k_ref.1, bf16[1024,128]{1,0:T(8,128)(2,1)} %v_ref.1, bf16[1024,128]{1,0:T(8,128)(2,1)} %d_ref.1, bf16[1024,128]{1,0:T(8,128)(2,1)} %b_ref.1, bf16[1024,128]{1,0:T(8,128)(2,1)} %gate_ref.1, ...), custom_call_target="tpu_custom_call" | custom-call | tf_op jit(solution)/shard_map/pallas_call | solution.py:730
  120.2 1.9 %copy.22 = bf16[128,2048]{1,0:T(8,128)(2,1)} copy(bf16[128,2048]{1,0:T(8,128)(2,1)} %get-tuple-element.4) | data formatting | bytes 1048576
  122.1 1.9 %copy.23 = bf16[128,2048]{1,0:T(8,128)(2,1)} copy(bf16[128,2048]{1,0:T(8,128)(2,1)} %get-tuple-element.5) | data formatting | bytes 1048576

commit v2 on v1

v2 whole, which is shorter than its diff:
```python
import functools

import jax
import jax.numpy as jnp
from jax import lax
from jax.experimental import pallas as pl
from jax.experimental.pallas import tpu as pltpu
from jax.sharding import PartitionSpec as P

HEAD_DIM = 64
BLOCK = 64


def dims(form):
    return {"nn": ((1,), (0,)), "nt": ((1,), (1,)), "tn": ((0,), (0,))}[form]


def mm1(left, right, form="nn"):
    return lax.dot_general(
        left.astype(jnp.bfloat16),
        right.astype(jnp.bfloat16),
        (dims(form), ((), ())),
        preferred_element_type=jnp.float32,
    )


def mm3(left, right, form="nn"):
    lh, rh = left.astype(jnp.bfloat16), right.astype(jnp.bfloat16)
    ll = (left - lh.astype(jnp.float32)).astype(jnp.bfloat16)
    rl = (right - rh.astype(jnp.float32)).astype(jnp.bfloat16)
    return mm1(lh, rh, form) + (mm1(lh, rl, form) + mm1(ll, rh, form))


mm_g = mm1
mm_inv = mm1
mm_q = mm1
mm_out = mm1
mm_car = mm1
mm_scan = mm1
mm_step = mm1
mm_fin = mm1


def head_masks(rows, width):
    lane = lax.broadcasted_iota(jnp.int32, (rows, width), 1)
    return lane < HEAD_DIM


def stacked(x):
    first = head_masks(*x.shape)
    return jnp.concatenate([jnp.where(first, x, 0.0), jnp.where(first, 0.0, x)], axis=0)


def per_head_sum(x):
    first = head_masks(*x.shape)
    one = jnp.sum(jnp.where(first, x, 0.0), axis=-1, keepdims=True)
    both = jnp.sum(jnp.where(first, 0.0, x), axis=-1, keepdims=True)
    return jnp.where(first, one, both)


def sigmoid(x):
    return 1.0 / (1.0 + jnp.exp(-x))


def block_stages(r_in, k_in, v_in, d_in, b_in):
    f32 = jnp.float32
    keys = k_in.astype(f32)
    unit = keys * lax.rsqrt(per_head_sum(keys * keys) + 1e-06)
    log_decay = sigmoid(d_in.astype(f32)) * -0.6065306597126334
    tri_row = lax.broadcasted_iota(jnp.int32, (BLOCK, 3 * BLOCK), 0)
    tri_col = lax.broadcasted_iota(jnp.int32, (BLOCK, 3 * BLOCK), 1) % BLOCK
    tri = jnp.where(tri_col <= tri_row, 1.0, 0.0).astype(jnp.bfloat16)
    hi = log_decay.astype(jnp.bfloat16)
    rest = log_decay - hi.astype(f32)
    mid = rest.astype(jnp.bfloat16)
    low = (rest - mid.astype(f32)).astype(jnp.bfloat16)
    cumul = mm1(tri, jnp.concatenate([hi, mid, low], axis=0))
    yield
    end_scale = jnp.exp(cumul[BLOCK - 1 :, :])
    shrink = jnp.exp(-cumul)
    query = r_in.astype(f32) * jnp.exp(cumul)
    alpha = -unit * jnp.exp(cumul - log_decay)
    key_grow = keys * shrink
    beta_grow = unit * sigmoid(b_in.astype(f32)) * shrink
    values = v_in.astype(f32)
    values2 = stacked(values)
    two = 2 * BLOCK
    grams = mm_g(
        jnp.concatenate([alpha, query], axis=0),
        jnp.concatenate([stacked(beta_grow), stacked(key_grow)], axis=0),
        "nt",
    )
    yield
    row = lax.broadcasted_iota(jnp.int32, (BLOCK, two), 0)
    col = lax.broadcasted_iota(jnp.int32, (BLOCK, two), 1) % BLOCK
    strict = col < row
    inclusive = col <= row
    couple = jnp.where(strict, grams[:BLOCK, :two], 0.0)
    insert = jnp.where(strict, grams[:BLOCK, two:], 0.0)
    read_beta = jnp.where(inclusive, grams[BLOCK:, :two], 0.0)
    read_key = jnp.where(inclusive, grams[BLOCK:, two:], 0.0)
    size = 8
    near = jnp.where(row // size == col // size, couple, 0.0)
    inverse = jnp.where(row == col, 1.0, 0.0) + near
    power = mm_inv(near, stacked(near))
    yield
    both = mm_inv(jnp.concatenate([inverse, power], axis=0), stacked(power))
    yield
    inverse = inverse + both[:BLOCK]
    inverse = inverse + mm_inv(inverse, stacked(both[BLOCK:]))
    yield
    while size < BLOCK:
        wide = 2 * size
        off = jnp.where(
            (row // wide == col // wide) & (row // size != col // size), couple, 0.0
        )
        step = mm_inv(off, stacked(inverse))
        yield
        inverse = inverse + mm_inv(inverse, stacked(step))
        yield
        size = wide
    inserted = mm_q(insert, values2)
    yield
    qz = mm_q(inverse, jnp.concatenate([stacked(alpha), stacked(inserted)], axis=1))
    yield
    q_rows, z_rows = qz[:, :two], qz[:, two:]
    upper = jnp.concatenate([stacked(q_rows), stacked(z_rows)], axis=1)
    lower = jnp.concatenate([jnp.zeros_like(values2), values2], axis=1)
    reads = mm_out(
        jnp.concatenate([read_beta, read_key], axis=1), jnp.concatenate([upper, lower], axis=0)
    )
    yield
    query_bar = query + reads[:, :two]
    local_out = reads[:, two:]
    ends = jnp.concatenate([beta_grow * end_scale, key_grow * end_scale], axis=0)
    lower = jnp.concatenate([jnp.zeros_like(values), values], axis=1)
    maps = mm_car(ends, jnp.concatenate([qz, lower], axis=0), "tn")
    yield
    head_row = lax.broadcasted_iota(jnp.int32, (two, 2 * two), 0) // HEAD_DIM
    head_col = lax.broadcasted_iota(jnp.int32, (two, 2 * two), 1) % two // HEAD_DIM
    maps = jnp.where(head_row == head_col, maps, 0.0)
    row = lax.broadcasted_iota(jnp.int32, (two, two), 0)
    col = lax.broadcasted_iota(jnp.int32, (two, two), 1)
    fade = jnp.sum(jnp.where(row == col, end_scale, 0.0), axis=1, keepdims=True)
    return query_bar, local_out, maps, fade


def local_blocks(inputs):
    stages = [block_stages(*block) for block in inputs]
    results = [None] * len(stages)
    while None in results:
        for i, stage in enumerate(stages):
            try:
                next(stage)
            except StopIteration as end:
                results[i] = end.value
    return results


def silu(x):
    return x / (1.0 + jnp.exp(-x))


def layer_kernel(
    unroll,
    pieces,
    slots,
    gain_ref,
    x_ref,
    moe_gain_ref,
    routes_ref,
    scores_ref,
    r_in,
    k_in,
    v_in,
    d_in,
    b_in,
    gate_in,
    project_in,
    expert_gate,
    expert_up,
    expert_down,
    shared_gate,
    shared_up,
    shared_down,
    mixed_ref,
    moe_ref,
    streams,
    state,
    qp_ref,
    lo_ref,
    rows_ref,
    totals,
    token_ref,
    project,
    weights,
    shared_one,
    shared_two,
    shared_three,
    shared_hidden,
    shared_term,
    others,
    other_routes,
    other_scores,
    normal,
    chosen_ref,
    spread_ref,
    leaving,
    arrived,
    returned,
    hidden_ref,
    part_out,
    part_in,
    table_send,
    table_recv,
    token_send,
    token_recv,
    slab_send,
    slab_recv,
    wide_send,
    wide_recv,
    pair_send,
    pair_recv,
    core_send,
    core_recv,
    relay_send,
    relay_recv,
    load_sem,
    stream_sem,
    go_send,
    go_recv,
    back_send,
    back_recv,
    part_send,
    part_recv,
    ep_send,
    ep_recv,
    row_send,
    row_recv,
):
    f32, bf16 = jnp.float32, jnp.bfloat16
    two = 2 * BLOCK
    MESH = pl.DeviceIdType.MESH
    stream_copies = [
        pltpu.make_async_copy(source, streams.at[i], stream_sem.at[i])
        for i, source in enumerate((r_in, k_in, v_in, d_in, b_in, gate_in))
    ]
    for copy in stream_copies:
        copy.start()
    here, mine = lax.axis_index("ep"), lax.axis_index("tp")
    groups, peers = lax.axis_size("ep"), lax.axis_size("tp")
    depth, core = mine // 2, mine % 2
    teams = peers // 4
    team, side = depth // 2, depth % 2
    seat = side * 2 + core
    facing = (1 - side) * 2 + core
    partner = depth * 2 + 1 - core
    across = team * 4 + facing
    tokens, width = x_ref.shape
    local, height = expert_gate.shape[0], expert_gate.shape[1]
    experts = local * groups
    span = local * slots
    columns = width // groups
    piece = width // pieces
    sources = (expert_gate, expert_up, expert_down)
    kinds = len(sources)
    cuts = kinds * local

    def remote(source, target, send, recv, device):
        return pltpu.make_async_remote_copy(
            src_ref=source,
            dst_ref=target,
            send_sem=send,
            recv_sem=recv,
            device_id=device,
            device_id_type=MESH,
        )

    def mate(shift):
        return {"tp": (team + shift) % teams * 4 + seat}

    def column(shift):
        return {"ep": (here + groups + shift) % groups}

    def table_copies(s):
        pairs = ((routes_ref, other_routes), (scores_ref, other_scores))
        return [
            remote(a, b.at[s], table_send.at[s, i], table_recv.at[s, i], mate(s))
            for i, (a, b) in enumerate(pairs)
        ]

    def token_copy(s, n):
        cols = pl.ds(pl.multiple_of(n * piece, piece), piece)
        return remote(
            normal.at[:, cols],
            others.at[s, :, cols],
            token_send.at[s, n],
            token_recv.at[s, n],
            mate(s),
        )

    def slab_place(owner, part):
        return project.at[
            pl.ds(pl.multiple_of(owner * two, two), two),
            pl.ds(pl.multiple_of(part * columns, columns), columns),
        ]

    def slab_copy(s):
        source = project_in.at[:, pl.ds(pl.multiple_of(here * columns, columns), columns)]
        target = mate(s) if s else {"tp": across}
        return remote(source, slab_place(mine, here), slab_send.at[s], slab_recv.at[s], target)

    def wide_copy(s, q):
        owner = (team + teams - s) % teams * 4 + seat if s else across
        block = slab_place(owner, here)
        return remote(block, block, wide_send.at[s, q], wide_recv.at[s, q], column(q))

    def weight_place(a, owner):
        return weights.at[a, pl.ds(pl.multiple_of(owner * height, height), height), :]

    def project_place(s, owner):
        base = (team + teams - s) % teams * 4 + owner
        return project.at[pl.ds(pl.multiple_of(base * two, two), two), :]

    def place_of(a, owner):
        return weight_place(a, owner) if a < cuts else project_place(a - cuts, owner)

    def own_block(a):
        if a < cuts:
            return sources[a % kinds].at[a // kinds]
        return project_in if a == cuts else project_place(a - cuts, seat)

    def pair_copy(a):
        return remote(
            own_block(a), place_of(a, seat), pair_send.at[a], pair_recv.at[a], {"tp": across}
        )

    def core_copy(a):
        return remote(
            own_block(a), place_of(a, seat), core_send.at[a], core_recv.at[a], {"tp": partner}
        )

    def relay_copy(a):
        block = place_of(a, facing)
        return remote(block, block, relay_send.at[a], relay_recv.at[a], {"tp": partner})

    def own_copy(a):
        return pltpu.make_async_copy(own_block(a), place_of(a, seat), load_sem.at[a])

    def relay(a):
        pair_copy(a).wait_recv()
        relay_copy(a).start()

    def ready(a):
        core_copy(a).wait_recv()
        relay_copy(a).wait_recv()

    def shared_copy(i):
        source = (shared_gate, shared_up, shared_down)[i]
        target = (shared_one, shared_two, shared_three)[i]
        return pltpu.make_async_copy(source, target, load_sem.at[cuts + 1 + i])

    def go_copy(s, q, n):
        cols = pl.ds(pl.multiple_of(n * piece, piece), piece)
        return remote(
            leaving.at[s, q, :, cols],
            arrived.at[s, q, :, cols],
            go_send.at[s, q, n],
            go_recv.at[s, q, n],
            column(q),
        )

    def back_copy(s, e, q, n):
        cols = pl.ds(pl.multiple_of(n * piece, piece), piece)
        return remote(
            arrived.at[s, q, pl.ds(e * slots, slots), cols],
            returned.at[s, q, pl.ds(e * slots, slots), cols],
            back_send.at[s, e, q, n],
            back_recv.at[s, e, q, n],
            column(-q),
        )

    def part_copy(s, n):
        cols = pl.ds(pl.multiple_of(n * piece, piece), piece)
        return remote(
            part_out.at[s, :, cols],
            part_in.at[s, :, cols],
            part_send.at[s, n],
            part_recv.at[s, n],
            mate(teams - s),
        )

    barrier = pltpu.get_barrier_semaphore()
    for q in range(1, peers):
        pl.semaphore_signal(
            barrier, inc=1, device_id={"tp": (mine + q) % peers}, device_id_type=MESH
        )
    for q in range(1, groups):
        pl.semaphore_signal(
            barrier, inc=1, device_id={"ep": (here + q) % groups}, device_id_type=MESH
        )
    def normalize():
        tall = 16

        def some(i, carry):
            rows = pl.ds(pl.multiple_of(i * tall, tall), tall)
            values = x_ref[rows, :].astype(f32)
            centered = values - jnp.sum(values, -1, keepdims=True) * (1.0 / width)
            spread = jnp.sum(centered * centered, -1, keepdims=True) * (1.0 / width)
            normal[rows, :] = (centered * lax.rsqrt(spread + 1e-05) * moe_gain_ref[...]).astype(
                bf16
            )
            return carry

        lax.fori_loop(0, tokens // tall, some, 0)

    def prepare(s, routes, scores):
        count = max(16, experts)
        order = lax.broadcasted_iota(jnp.int32, (count, tokens), 0)
        names = (here + order // local) % groups * local + order % local
        names = jnp.where(order < experts, names, -1)
        tops = routes.shape[0]
        hits = [routes[k : k + 1, :] == names for k in range(tops)]
        picks = sum(jnp.where(hit, 1.0, 0.0) for hit in hits)
        past = lax.broadcasted_iota(jnp.int32, (tokens, tokens), 0)
        present = lax.broadcasted_iota(jnp.int32, (tokens, tokens), 1)
        earlier = mm1(picks, jnp.where(past < present, 1.0, 0.0))
        index = order.astype(f32) * slots + earlier
        row = lax.broadcasted_iota(jnp.int32, (experts * slots, tokens), 0).astype(f32)
        match = [
            row == jnp.sum(jnp.where(hit, index, 0.0), axis=0, keepdims=True) for hit in hits
        ]
        total = sum(scores[k : k + 1, :] for k in range(tops))
        chosen_ref[...] = sum(jnp.where(m, 1.0, 0.0) for m in match).astype(bf16)
        spread = sum(
            jnp.where(match[k], 2.5 * scores[k : k + 1, :] / total, 0.0) for k in range(tops)
        )
        spread_ref[s] = jnp.transpose(spread).astype(bf16)

    def dispatch(s, n, source):
        half = piece // 2
        for i in range(2):
            cols = pl.ds(pl.multiple_of(n * piece + i * half, half), half)
            out = jnp.dot(chosen_ref[...], source[:, cols], preferred_element_type=f32).astype(bf16)
            arrived[s, 0, :, cols] = out[:span]
            leaving[s, 1:, :, cols] = out[span:].reshape(groups - 1, span, half)

        def send(q, carry):
            go_copy(s, q, n).start()
            return carry

        lax.fori_loop(1, groups, send, 0)

    normalize()
    prepare(0, routes_ref, scores_ref)
    pl.semaphore_wait(barrier, peers + groups - 2)

    for s in range(1, teams):
        for copy in table_copies(s):
            copy.start()
        for n in range(pieces):
            token_copy(s, n).start()
    for s in range(teams):
        slab_copy(s).start()
    for a in range(cuts + 1):
        if a < cuts:
            pair_copy(a).start()
        core_copy(a).start()
        own_copy(a).start()
    for i in range(3):
        shared_copy(i).start()

    def own_piece(n, carry):
        dispatch(0, n, normal)
        return carry

    lax.fori_loop(0, pieces, own_piece, 0)
    for copy in stream_copies:
        copy.wait()
    r_ref, k_ref, v_ref, d_ref, b_ref, gate_ref = (streams.at[i] for i in range(6))

    row = lax.broadcasted_iota(jnp.int32, (two, 2 * two), 0)
    col = lax.broadcasted_iota(jnp.int32, (two, 2 * two), 1)
    state[...] = jnp.where(row == col, 1.0, 0.0)
    turns = r_ref.shape[0] // (BLOCK * unroll)

    def turn(step, carry):
        places = [
            pl.ds(pl.multiple_of((step * unroll + u) * BLOCK, BLOCK), BLOCK) for u in range(unroll)
        ]
        parts = local_blocks(
            [[ref[rows, :] for ref in (r_ref, k_ref, v_ref, d_ref, b_ref)] for rows in places]
        )
        now = state[...]
        for rows, (query_bar, local_out, maps, fade) in zip(places, parts):
            out = mm_scan(query_bar, now)
            qp_ref[rows, :] = out[:, :two]
            lo_ref[rows, :] = out[:, two:] + local_out
            moved = mm_step(maps[:, :two], now) + now * fade
            now = jnp.concatenate([moved[:, :two], moved[:, two:] + maps[:, two:]], axis=1)
        state[...] = now
        return carry

    lax.fori_loop(0, turns, turn, 0)

    carry_map, source_map = state[:, :two], state[:, two:]
    totals[here, 0] = (carry_map[:BLOCK] + carry_map[BLOCK:]).astype(totals.dtype)
    totals[here, 1] = (source_map[:BLOCK] + source_map[BLOCK:]).astype(totals.dtype)

    def ep_copy(q, slot):
        return remote(
            totals.at[slot], totals.at[slot], ep_send.at[q], ep_recv.at[q], column(q)
        )

    for q in range(1, groups):
        ep_copy(q, here).start()

    def widen(s):
        slab_copy(s).wait_recv()

        def each(q, carry):
            wide_copy(s, q).start()
            return carry

        lax.fori_loop(1, groups, each, 0)

    def widened(s):
        def each(q, carry):
            wide_copy(s, q).wait_recv()
            return carry

        lax.fori_loop(1, groups, each, 0)

    def receive(s, carry):
        for copy in table_copies(s):
            copy.wait_recv()
        prepare(s, other_routes.at[s], other_scores.at[s])

        def other_piece(n, inner):
            token_copy(s, n).wait_recv()
            dispatch(s, n, others.at[s])
            return inner

        return lax.fori_loop(0, pieces, other_piece, carry)

    lax.fori_loop(1, teams, receive, 0)

    for s in range(teams):
        widen(s)

    for i in range(3):
        shared_copy(i).wait()
    step = 256
    for i in range(shared_one.shape[1] // step):
        cols = slice(i * step, (i + 1) * step)
        gate = jnp.dot(normal[...], shared_one[:, cols], preferred_element_type=f32)
        upper = jnp.dot(normal[...], shared_two[:, cols], preferred_element_type=f32)
        shared_hidden[:, cols] = (silu(gate) * upper).astype(bf16)

    def share(i, carry):
        cols = pl.ds(pl.multiple_of(i * step, step), step)
        shared_term[:, cols] = jnp.dot(
            shared_hidden[...], shared_three[:, cols], preferred_element_type=f32
        )
        return carry

    lax.fori_loop(0, width // step, share, 0)

    for q in range(1, groups):
        ep_copy(q, (here + groups - q) % groups).wait_recv()

    def enter(k, entry):
        carry = stacked(totals[k, 0].astype(f32))
        source = stacked(totals[k, 1].astype(f32))
        reached = jnp.where(k < here, 1.0, 0.0)
        return entry + reached * (mm3(carry, entry) + source - entry)

    entry = lax.fori_loop(0, groups, enter, jnp.zeros((two, two), f32))

    def row_copy(q, target, source):
        return remote(
            rows_ref.at[pl.ds(pl.multiple_of(target * tokens, tokens), tokens), :],
            token_ref.at[:, pl.ds(pl.multiple_of(source * two, two), two)],
            row_send.at[q],
            row_recv.at[q],
            {"tp": target},
        )

    def finish(rows):
        recur = mm_fin(qp_ref[rows, :], entry) + lo_ref[rows, :]
        centered = recur - per_head_sum(recur) * (1.0 / HEAD_DIM)
        spread = per_head_sum(centered * centered) * (1.0 / HEAD_DIM)
        normed = centered * lax.rsqrt(spread + 0.00064)
        gated = normed * gain_ref[...] * sigmoid(gate_ref[rows, :].astype(f32))
        rows_ref[rows, :] = gated.astype(bf16)

    def finish_turn(q, carry):
        finish(pl.ds(pl.multiple_of(q * tokens, tokens), tokens))
        return carry

    lax.fori_loop(0, peers, finish_turn, 0)
    own_rows = pltpu.make_async_copy(
        rows_ref.at[pl.ds(pl.multiple_of(mine * tokens, tokens), tokens), :],
        token_ref.at[:, pl.ds(pl.multiple_of(mine * two, two), two)],
        load_sem.at[cuts + 4],
    )
    own_rows.start()

    def row_start(q, carry):
        row_copy(q, (mine + q) % peers, mine).start()
        return carry

    lax.fori_loop(1, peers, row_start, 0)

    nt = (((1,), (1,)), ((), ()))

    def feed(s, e):
        mine_slots = pl.ds(e * slots, slots)
        x = arrived[s, :, mine_slots, :].reshape(groups * slots, width)
        gate = lax.dot_general(x, weights[e * kinds], nt, preferred_element_type=f32)
        upper = lax.dot_general(x, weights[e * kinds + 1], nt, preferred_element_type=f32)
        hidden_ref[...] = (silu(gate) * upper).astype(bf16)

        def down(n, carry):
            cols = pl.ds(pl.multiple_of(n * piece, piece), piece)
            out = jnp.dot(
                hidden_ref[...], weights[e * kinds + 2, :, cols], preferred_element_type=f32
            )
            out = out.astype(bf16).reshape(groups, slots, piece)
            returned[s, 0, mine_slots, cols] = out[0]
            arrived[s, 1:, mine_slots, cols] = out[1:]

            def back(q, inner):
                back_copy(s, e, q, n).start()
                return inner

            return lax.fori_loop(1, groups, back, carry)

        lax.fori_loop(0, pieces, down, 0)

    def come(s):
        def each(q, carry):
            def some(n, inner):
                go_copy(s, q, n).wait_recv()
                return inner

            return lax.fori_loop(0, pieces, some, carry)

        lax.fori_loop(1, groups, each, 0)

    def have(e):
        for a in range(e * kinds, (e + 1) * kinds):
            relay(a)
        for a in range(e * kinds, (e + 1) * kinds):
            own_copy(a).wait()
            ready(a)

    for e in range(local):
        have(e)

        def mates(s, carry, e=e):
            if e == 0:
                come(s)
            feed(s, e)
            return carry

        lax.fori_loop(1, teams, mates, 0)
        if e == 0:
            for s in range(1, teams):
                widened(s)
                pair_copy(cuts + s).start()
                core_copy(cuts + s).start()
            widened(0)
            relay_copy(cuts).start()
    come(0)

    def mine_too(e, carry):
        feed(0, e)
        return carry

    lax.fori_loop(0, local, mine_too, 0)

    def combined(s, n):
        def each(q, carry):
            for e in range(local):
                back_copy(s, e, q, n).wait_recv()
            return carry

        lax.fori_loop(1, groups, each, 0)
        cols = pl.ds(pl.multiple_of(n * piece, piece), piece)
        rows = returned[s, :, :, cols].reshape(groups * span, piece)
        return jnp.dot(spread_ref[s], rows, preferred_element_type=f32), cols

    def partial(s, carry):
        def some(n, inner):
            value, cols = combined(s, n)
            part_out[s, :, cols] = value.astype(bf16)
            part_copy(s, n).start()
            return inner

        return lax.fori_loop(0, pieces, some, carry)

    lax.fori_loop(1, teams, partial, 0)

    for a in range(cuts + 1, cuts + teams):
        relay(a)
    own_copy(cuts).wait()
    for a in range(cuts, cuts + teams):
        ready(a)
    own_rows.wait()

    def row_end(q, carry):
        row_copy(q, (mine + q) % peers, (mine + peers - q) % peers).wait()
        return carry

    lax.fori_loop(1, peers, row_end, 0)

    def mix(i, carry):
        cols = pl.ds(pl.multiple_of(i * step, step), step)
        mixed_ref[:, cols] = jnp.dot(
            token_ref[...], project[:, cols], preferred_element_type=f32
        ).astype(bf16)
        return carry

    lax.fori_loop(0, width // step, mix, 0)

    def close(n, carry):
        value, cols = combined(0, n)
        total = value + shared_term[:, cols]
        for s in range(1, teams):
            part_copy(s, n).wait_recv()
            total = total + part_in[s, :, cols].astype(f32)
        moe_ref[:, cols] = total.astype(bf16)
        return carry

    lax.fori_loop(0, pieces, close, 0)

    for a in range(cuts + teams):
        if a != cuts:
            pair_copy(a).wait_send()
        core_copy(a).wait_send()
        relay_copy(a).wait_send()
    for q in range(1, groups):
        ep_copy(q, here).wait_send()

    def sent(s, carry):
        def each(q, inner):
            def block(n, last):
                go_copy(s, q, n).wait_send()
                for e in range(local):
                    back_copy(s, e, q, n).wait_send()
                return last

            return lax.fori_loop(0, pieces, block, inner)

        return lax.fori_loop(1, groups, each, carry)

    lax.fori_loop(0, teams, sent, 0)

    def shipped(s, carry):
        for copy in table_copies(s):
            copy.wait_send()

        def block(n, inner):
            part_copy(s, n).wait_send()
            token_copy(s, n).wait_send()
            return inner

        return lax.fori_loop(0, pieces, block, carry)

    lax.fori_loop(1, teams, shipped, 0)
    for s in range(teams):
        slab_copy(s).wait_send()

        def spread_out(q, carry, s=s):
            wide_copy(s, q).wait_send()
            return carry

        lax.fori_loop(1, groups, spread_out, 0)


def shards(
    receptance,
    key_in,
    payload_vectors,
    decay_in,
    rate_in,
    gate_in,
    norm_gain,
    out_weight,
    moe_in,
    moe_gain,
    routes,
    route_weights,
    expert_gate,
    expert_up,
    expert_down,
    shared_gate,
    shared_up,
    shared_down,
):
    length, channels = receptance.shape
    tokens, width = moe_in.shape
    groups, peers = lax.axis_size("ep"), lax.axis_size("tp")
    teams = peers // 4
    local, _, height = expert_gate.shape
    top_count = routes.shape[1]
    experts = local * groups
    slots = max(2, 3 * tokens * top_count // (2 * experts))
    slots = -(-slots // 16) * 16
    span = local * slots
    inner = shared_gate.shape[1]
    pieces = 4
    kinds = 3
    wide = 2 * HEAD_DIM
    spare = wide - channels
    pad = lambda x: jnp.pad(x, ((0, 0),) * (x.ndim - 1) + ((0, spare),)) if spare else x
    weight_rows = jnp.pad(out_weight, ((0, spare), (0, 0))) if spare else out_weight
    f32, bf16 = jnp.float32, jnp.bfloat16
    vmem = pl.BlockSpec(memory_space=pltpu.VMEM)
    anywhere = pl.BlockSpec(memory_space=pl.ANY)
    dma = pltpu.SemaphoreType.DMA
    out = jax.ShapeDtypeStruct((tokens, width), bf16)
    turned = lambda w: jnp.swapaxes(w, 1, 2)
    return pl.pallas_call(
        functools.partial(layer_kernel, 8, pieces, slots),
        out_shape=(out, out),
        in_specs=[vmem] * 5 + [anywhere] * 13,
        out_specs=(vmem, vmem),
        scratch_shapes=[
            pltpu.VMEM((6, length, wide), bf16),
            pltpu.VMEM((wide, 2 * wide), f32),
            pltpu.VMEM((length, wide), f32),
            pltpu.VMEM((length, wide), f32),
            pltpu.VMEM((length, wide), bf16),
            pltpu.VMEM((groups, 2, HEAD_DIM, wide), bf16),
            pltpu.VMEM((tokens, peers * wide), bf16),
            pltpu.VMEM((peers * wide, width), bf16),
            pltpu.VMEM((kinds * local, 4 * height, width), bf16),
            pltpu.VMEM(shared_gate.shape, bf16),
            pltpu.VMEM(shared_up.shape, bf16),
            pltpu.VMEM(shared_down.shape, bf16),
            pltpu.VMEM((tokens, inner), bf16),
            pltpu.VMEM((tokens, width), f32),
            pltpu.VMEM((teams, tokens, width), bf16),
            pltpu.VMEM((teams, top_count, tokens), jnp.int32),
            pltpu.VMEM((teams, top_count, tokens), f32),
            pltpu.VMEM((tokens, width), bf16),
            pltpu.VMEM((experts * slots, tokens), bf16),
            pltpu.VMEM((teams, tokens, experts * slots), bf16),
            pltpu.VMEM((teams, groups, span, width), bf16),
            pltpu.VMEM((teams, groups, span, width), bf16),
            pltpu.VMEM((teams, groups, span, width), bf16),
            pltpu.VMEM((groups * slots, 4 * height), bf16),
            pltpu.VMEM((teams, tokens, width), bf16),
            pltpu.VMEM((teams, tokens, width), bf16),
            dma((teams, 2)),
            dma((teams, 2)),
            dma((teams, pieces)),
            dma((teams, pieces)),
            dma((teams,)),
            dma((teams,)),
            dma((teams, groups)),
            dma((teams, groups)),
            dma((kinds * local + teams,)),
            dma((kinds * local + teams,)),
            dma((kinds * local + teams,)),
            dma((kinds * local + teams,)),
            dma((kinds * local + teams,)),
            dma((kinds * local + teams,)),
            dma((kinds * local + 5,)),
            dma((6,)),
            dma((teams, groups, pieces)),
            dma((teams, groups, pieces)),
            dma((teams, local, groups, pieces)),
            dma((teams, local, groups, pieces)),
            dma((teams, pieces)),
            dma((teams, pieces)),
            dma((groups,)),
            dma((groups,)),
            dma((peers,)),
            dma((peers,)),
        ],
        compiler_params=pltpu.CompilerParams(
            collective_id=0, has_side_effects=True, vmem_limit_bytes=63 << 20
        ),
    )(
        pad(norm_gain).reshape(1, wide),
        moe_in,
        moe_gain.reshape(1, width),
        routes.T,
        route_weights.T,
        pad(receptance),
        pad(key_in),
        pad(payload_vectors),
        pad(decay_in),
        pad(rate_in),
        pad(gate_in),
        weight_rows,
        turned(expert_gate),
        turned(expert_up),
        turned(expert_down),
        shared_gate,
        shared_up,
        shared_down,
    )


def solution(mesh):
    placed = (
        P("ep", "tp"),
        P("ep", "tp"),
        P("ep", "tp"),
        P("ep", "tp"),
        P("ep", "tp"),
        P("ep", "tp"),
        P("tp"),
        P("tp", None),
        P(("ep", "tp"), None),
        P(),
        P(("ep", "tp"), None),
        P(("ep", "tp"), None),
        P("ep", None, "tp"),
        P("ep", None, "tp"),
        P("ep", None, "tp"),
        P(),
        P(),
        P(),
    )
    return jax.shard_map(
        shards,
        mesh=mesh,
        in_specs=placed,
        out_specs=(P(("ep", "tp"), None), P(("ep", "tp"), None)),
        check_vma=False,
    )
```

time: 124 us -> 101 us (0.81)
  Pallas kernels: 120 us -> 96.6 us
    pallas_call x1, Pallas kernels: 120 us -> 96.6 us  [shards(): pl.pallas_call(functools.partial(layer_kernel, 8, pieces, slots), out_sha...]
where the time goes in v2:
time: 101 us
  Pallas kernels  96.6 us (96%)
  local copies, waits for them, and re-layouts  3.76 us (4%)
    pallas_call x1, Pallas kernels, shards(): pl.pallas_call(functools.partial(layer_kernel, 8, pieces, slots), out_sha...  96.6 us
    unnamed x2, local copies, waits for them, and re-layouts  3.76 us

profile of v2, /device:TPU:0, one launch (start us, length us, event | category | flops | bytes accessed | tf_op | source)
XLA Modules:
  0.0 101.0 jit_solution(4951140371092447901)
XLA Ops:
  0.6 96.6 %shard_map.185 = (bf16[128,2048]{1,0:T(8,128)(2,1)}, bf16[128,2048]{1,0:T(8,128)(2,1)}) custom-call(f32[1,128]{1,0:T(1,128)} %bitcast.13, bf16[128,2048]{1,0:T(8,128)(2,1)} %x_ref.1, f32[1,2048]{1,0:T(1,128)} %bitcast.10, s32[2,128]{1,0:T(2,128)} %bitcast.11, f32[2,128]{1,0:T(2,128)} %bitcast.12, bf16[1024,128]{1,0:T(8,128)(2,1)} %r_in.1, ...), custom_call_target="tpu_custom_call" | custom-call | tf_op jit(solution)/shard_map/pallas_call | solution.py:825
  97.3 1.9 %copy.22 = bf16[128,2048]{1,0:T(8,128)(2,1)} copy(bf16[128,2048]{1,0:T(8,128)(2,1)} %get-tuple-element.4) | data formatting | bytes 1048576
  99.1 1.9 %copy.23 = bf16[128,2048]{1,0:T(8,128)(2,1)} copy(bf16[128,2048]{1,0:T(8,128)(2,1)} %get-tuple-element.5) | data formatting | bytes 1048576

commit v3 on v2

--- a/solution.py
+++ b/solution.py
@@ -165,11 +165,11 @@
     unroll,
     pieces,
     slots,
-    gain_ref,
-    x_ref,
-    moe_gain_ref,
-    routes_ref,
-    scores_ref,
+    gain_in,
+    x_in,
+    moe_gain_in,
+    routes_in,
+    scores_in,
     r_in,
     k_in,
     v_in,
@@ -185,6 +185,11 @@
     shared_down,
     mixed_ref,
     moe_ref,
+    x_ref,
+    moe_gain_ref,
+    routes_ref,
+    scores_ref,
+    gain_ref,
     streams,
     state,
     qp_ref,
@@ -194,6 +199,7 @@
     token_ref,
     project,
     weights,
+    downs,
     shared_one,
     shared_two,
     shared_three,
@@ -241,11 +247,22 @@
     f32, bf16 = jnp.float32, jnp.bfloat16
     two = 2 * BLOCK
     MESH = pl.DeviceIdType.MESH
+    first_pairs = (
+        (x_in, x_ref),
+        (moe_gain_in, moe_gain_ref),
+        (routes_in, routes_ref),
+        (scores_in, scores_ref),
+        (gain_in, gain_ref),
+    )
+    first_copies = [
+        pltpu.make_async_copy(source, target, stream_sem.at[6 + i])
+        for i, (source, target) in enumerate(first_pairs)
+    ]
     stream_copies = [
         pltpu.make_async_copy(source, streams.at[i], stream_sem.at[i])
         for i, source in enumerate((r_in, k_in, v_in, d_in, b_in, gate_in))
     ]
-    for copy in stream_copies:
+    for copy in first_copies + stream_copies:
         copy.start()
     here, mine = lax.axis_index("ep"), lax.axis_index("tp")
     groups, peers = lax.axis_size("ep"), lax.axis_size("tp")
@@ -256,15 +273,15 @@
     facing = (1 - side) * 2 + core
     partner = depth * 2 + 1 - core
     across = team * 4 + facing
-    tokens, width = x_ref.shape
+    tokens, width = x_in.shape
     local, height = expert_gate.shape[0], expert_gate.shape[1]
     experts = local * groups
     span = local * slots
     columns = width // groups
     piece = width // pieces
-    sources = (expert_gate, expert_up, expert_down)
-    kinds = len(sources)
-    cuts = kinds * local
+    sources = (expert_gate, expert_up)
+    firsts = 2 * local
+    cuts = firsts + pieces
 
     def remote(source, target, send, recv, device):
         return pltpu.make_async_remote_copy(
@@ -310,13 +327,32 @@
         target = mate(s) if s else {"tp": across}
         return remote(source, slab_place(mine, here), slab_send.at[s], slab_recv.at[s], target)
 
-    def wide_copy(s, q):
+    bits = groups.bit_length() - 1
+
+    def flipped(mask):
+        place = here
+        for i in range(bits):
+            if mask >> i & 1:
+                place = place + (1 << i) * (1 - here // (1 << i) % 2 * 2)
+        return place
+
+    def wide_copy(s, k, j):
         owner = (team + teams - s) % teams * 4 + seat if s else across
-        block = slab_place(owner, here)
-        return remote(block, block, wide_send.at[s, q], wide_recv.at[s, q], column(q))
+        order = [(i + s) % bits for i in range(bits)]
+        mask = sum((j >> i & 1) << order[i] for i in range(k))
+        block = slab_place(owner, flipped(mask))
+        slot = (1 << k) + j
+        target = {"ep": flipped(1 << order[k])}
+        return remote(block, block, wide_send.at[s, slot], wide_recv.at[s, slot], target)
+
+    def wide_copies(s, k):
+        return [wide_copy(s, k, j) for j in range(1 << k)]
 
     def weight_place(a, owner):
-        return weights.at[a, pl.ds(pl.multiple_of(owner * height, height), height), :]
+        rows = pl.ds(pl.multiple_of(owner * height, height), height)
+        if a < firsts:
+            return weights.at[a, rows, :]
+        return downs.at[:, rows, pl.ds((a - firsts) * piece, piece)]
 
     def project_place(s, owner):
         base = (team + teams - s) % teams * 4 + owner
@@ -326,8 +362,10 @@
         return weight_place(a, owner) if a < cuts else project_place(a - cuts, owner)
 
     def own_block(a):
+        if a < firsts:
+            return sources[a % 2].at[a // 2]
         if a < cuts:
-            return sources[a % kinds].at[a // kinds]
+            return expert_down.at[:, :, pl.ds((a - firsts) * piece, piece)]
         return project_in if a == cuts else project_place(a - cuts, seat)
 
     def pair_copy(a):
@@ -370,13 +408,13 @@
             column(q),
         )
 
-    def back_copy(s, e, q, n):
+    def back_copy(s, q, n):
         cols = pl.ds(pl.multiple_of(n * piece, piece), piece)
         return remote(
-            arrived.at[s, q, pl.ds(e * slots, slots), cols],
-            returned.at[s, q, pl.ds(e * slots, slots), cols],
-            back_send.at[s, e, q, n],
-            back_recv.at[s, e, q, n],
+            arrived.at[s, q, :, cols],
+            returned.at[s, q, :, cols],
+            back_send.at[s, q, n],
+            back_recv.at[s, q, n],
             column(-q),
         )
 
@@ -451,6 +489,8 @@
 
         lax.fori_loop(1, groups, send, 0)
 
+    for copy in first_copies:
+        copy.wait()
     normalize()
     prepare(0, routes_ref, scores_ref)
     pl.semaphore_wait(barrier, peers + groups - 2)
@@ -515,21 +555,17 @@
     for q in range(1, groups):
         ep_copy(q, here).start()
 
-    def widen(s):
-        slab_copy(s).wait_recv()
-
-        def each(q, carry):
-            wide_copy(s, q).start()
-            return carry
-
-        lax.fori_loop(1, groups, each, 0)
-
-    def widened(s):
-        def each(q, carry):
-            wide_copy(s, q).wait_recv()
-            return carry
-
-        lax.fori_loop(1, groups, each, 0)
+    def widened(s, k):
+        for copy in wide_copies(s, k):
+            copy.wait_recv()
+
+    def widen(s, k):
+        if k:
+            widened(s, k - 1)
+        else:
+            slab_copy(s).wait_recv()
+        for copy in wide_copies(s, k):
+            copy.start()
 
     def receive(s, carry):
         for copy in table_copies(s):
@@ -546,7 +582,7 @@
     lax.fori_loop(1, teams, receive, 0)
 
     for s in range(teams):
-        widen(s)
+        widen(s, 0)
 
     for i in range(3):
         shared_copy(i).wait()
@@ -599,91 +635,93 @@
         return carry
 
     lax.fori_loop(0, peers, finish_turn, 0)
+    nt = (((1,), (1,)), ((), ()))
+
+    def enlarge(s, carry):
+        come(s)
+        for e in range(local):
+            x = arrived[s, :, pl.ds(e * slots, slots), :].reshape(groups * slots, width)
+            gate = lax.dot_general(x, weights[2 * e], nt, preferred_element_type=f32)
+            upper = lax.dot_general(x, weights[2 * e + 1], nt, preferred_element_type=f32)
+            hidden_ref[s, e] = (silu(gate) * upper).astype(bf16)
+        return carry
+
+    def reduce(s, n):
+        cols = pl.ds(pl.multiple_of(n * piece, piece), piece)
+        for e in range(local):
+            mine_slots = pl.ds(e * slots, slots)
+            out = jnp.dot(hidden_ref[s, e], downs[e, :, cols], preferred_element_type=f32)
+            out = out.astype(bf16).reshape(groups, slots, piece)
+            returned[s, 0, mine_slots, cols] = out[0]
+            arrived[s, 1:, mine_slots, cols] = out[1:]
+
+        def back(q, carry):
+            back_copy(s, q, n).start()
+            return carry
+
+        lax.fori_loop(1, groups, back, 0)
+
+    def come(s):
+        def each(q, carry):
+            def some(n, inner):
+                go_copy(s, q, n).wait_recv()
+                return inner
+
+            return lax.fori_loop(0, pieces, some, carry)
+
+        lax.fori_loop(1, groups, each, 0)
+
+    for a in range(firsts):
+        relay(a)
+        if a == firsts - 2:
+            for k in range(1, bits):
+                for s in range(teams):
+                    widen(s, k)
+    for a in range(firsts):
+        own_copy(a).wait()
+        ready(a)
+    lax.fori_loop(1, teams, enlarge, 0)
     own_rows = pltpu.make_async_copy(
         rows_ref.at[pl.ds(pl.multiple_of(mine * tokens, tokens), tokens), :],
         token_ref.at[:, pl.ds(pl.multiple_of(mine * two, two), two)],
         load_sem.at[cuts + 4],
     )
-    own_rows.start()
 
     def row_start(q, carry):
         row_copy(q, (mine + q) % peers, mine).start()
         return carry
 
+    own_rows.start()
     lax.fori_loop(1, peers, row_start, 0)
-
-    nt = (((1,), (1,)), ((), ()))
-
-    def feed(s, e):
-        mine_slots = pl.ds(e * slots, slots)
-        x = arrived[s, :, mine_slots, :].reshape(groups * slots, width)
-        gate = lax.dot_general(x, weights[e * kinds], nt, preferred_element_type=f32)
-        upper = lax.dot_general(x, weights[e * kinds + 1], nt, preferred_element_type=f32)
-        hidden_ref[...] = (silu(gate) * upper).astype(bf16)
-
-        def down(n, carry):
-            cols = pl.ds(pl.multiple_of(n * piece, piece), piece)
-            out = jnp.dot(
-                hidden_ref[...], weights[e * kinds + 2, :, cols], preferred_element_type=f32
-            )
-            out = out.astype(bf16).reshape(groups, slots, piece)
-            returned[s, 0, mine_slots, cols] = out[0]
-            arrived[s, 1:, mine_slots, cols] = out[1:]
-
-            def back(q, inner):
-                back_copy(s, e, q, n).start()
-                return inner
-
-            return lax.fori_loop(1, groups, back, carry)
-
-        lax.fori_loop(0, pieces, down, 0)
-
-    def come(s):
-        def each(q, carry):
-            def some(n, inner):
-                go_copy(s, q, n).wait_recv()
-                return inner
-
-            return lax.fori_loop(0, pieces, some, carry)
-
-        lax.fori_loop(1, groups, each, 0)
-
-    def have(e):
-        for a in range(e * kinds, (e + 1) * kinds):
-            relay(a)
-        for a in range(e * kinds, (e + 1) * kinds):
-            own_copy(a).wait()
-            ready(a)
-
-    for e in range(local):
-        have(e)
-
-        def mates(s, carry, e=e):
-            if e == 0:
-                come(s)
-            feed(s, e)
+    for n in range(pieces):
+        a = firsts + n
+        relay(a)
+        own_copy(a).wait()
+        ready(a)
+
+        def mates(s, carry, n=n):
+            reduce(s, n)
             return carry
 
         lax.fori_loop(1, teams, mates, 0)
-        if e == 0:
+        if n == pieces // 2:
             for s in range(1, teams):
-                widened(s)
+                widened(s, bits - 1)
                 pair_copy(cuts + s).start()
                 core_copy(cuts + s).start()
-            widened(0)
-            relay_copy(cuts).start()
-    come(0)
-
-    def mine_too(e, carry):
-        feed(0, e)
+
+    enlarge(0, 0)
+
+    def mine_too(n, carry):
+        reduce(0, n)
         return carry
 
-    lax.fori_loop(0, local, mine_too, 0)
-
+    lax.fori_loop(0, pieces, mine_too, 0)
+    widened(0, bits - 1)
+    relay_copy(cuts).start()
     def combined(s, n):
         def each(q, carry):
-            for e in range(local):
-                back_copy(s, e, q, n).wait_recv()
+            back_copy(s, q, n).wait_recv()
             return carry
 
         lax.fori_loop(1, groups, each, 0)
@@ -747,8 +785,7 @@
         def each(q, inner):
             def block(n, last):
                 go_copy(s, q, n).wait_send()
-                for e in range(local):
-                    back_copy(s, e, q, n).wait_send()
+                back_copy(s, q, n).wait_send()
                 return last
 
             return lax.fori_loop(0, pieces, block, inner)
@@ -771,12 +808,9 @@
     lax.fori_loop(1, teams, shipped, 0)
     for s in range(teams):
         slab_copy(s).wait_send()
-
-        def spread_out(q, carry, s=s):
-            wide_copy(s, q).wait_send()
-            return carry
-
-        lax.fori_loop(1, groups, spread_out, 0)
+        for k in range(bits):
+            for copy in wide_copies(s, k):
+                copy.wait_send()
 
 
 def shards(
@@ -811,7 +845,7 @@
     span = local * slots
     inner = shared_gate.shape[1]
     pieces = 4
-    kinds = 3
+    cuts = 2 * local + pieces
     wide = 2 * HEAD_DIM
     spare = wide - channels
     pad = lambda x: jnp.pad(x, ((0, 0),) * (x.ndim - 1) + ((0, spare),)) if spare else x
@@ -820,14 +854,19 @@
     vmem = pl.BlockSpec(memory_space=pltpu.VMEM)
     anywhere = pl.BlockSpec(memory_space=pl.ANY)
     dma = pltpu.SemaphoreType.DMA
-    out = jax.ShapeDtypeStruct((tokens, width), bf16)
+    out = pltpu.VMEM((tokens, width), bf16)
     turned = lambda w: jnp.swapaxes(w, 1, 2)
     return pl.pallas_call(
         functools.partial(layer_kernel, 8, pieces, slots),
         out_shape=(out, out),
-        in_specs=[vmem] * 5 + [anywhere] * 13,
+        in_specs=[anywhere] * 18,
         out_specs=(vmem, vmem),
         scratch_shapes=[
+            pltpu.VMEM((tokens, width), bf16),
+            pltpu.VMEM((1, width), f32),
+            pltpu.VMEM((top_count, tokens), jnp.int32),
+            pltpu.VMEM((top_count, tokens), f32),
+            pltpu.VMEM((1, wide), f32),
             pltpu.VMEM((6, length, wide), bf16),
             pltpu.VMEM((wide, 2 * wide), f32),
             pltpu.VMEM((length, wide), f32),
@@ -836,7 +875,8 @@
             pltpu.VMEM((groups, 2, HEAD_DIM, wide), bf16),
             pltpu.VMEM((tokens, peers * wide), bf16),
             pltpu.VMEM((peers * wide, width), bf16),
-            pltpu.VMEM((kinds * local, 4 * height, width), bf16),
+            pltpu.VMEM((2 * local, 4 * height, width), bf16),
+            pltpu.VMEM((local, 4 * height, width), bf16),
             pltpu.VMEM(shared_gate.shape, bf16),
             pltpu.VMEM(shared_up.shape, bf16),
             pltpu.VMEM(shared_down.shape, bf16),
@@ -851,7 +891,7 @@
             pltpu.VMEM((teams, groups, span, width), bf16),
             pltpu.VMEM((teams, groups, span, width), bf16),
             pltpu.VMEM((teams, groups, span, width), bf16),
-            pltpu.VMEM((groups * slots, 4 * height), bf16),
+            pltpu.VMEM((teams, local, groups * slots, 4 * height), bf16),
             pltpu.VMEM((teams, tokens, width), bf16),
             pltpu.VMEM((teams, tokens, width), bf16),
             dma((teams, 2)),
@@ -862,18 +902,18 @@
             dma((teams,)),
             dma((teams, groups)),
             dma((teams, groups)),
-            dma((kinds * local + teams,)),
-            dma((kinds * local + teams,)),
-            dma((kinds * local + teams,)),
-            dma((kinds * local + teams,)),
-            dma((kinds * local + teams,)),
-            dma((kinds * local + teams,)),
-            dma((kinds * local + 5,)),
-            dma((6,)),
+            dma((cuts + teams,)),
+            dma((cuts + teams,)),
+            dma((cuts + teams,)),
+            dma((cuts + teams,)),
+            dma((cuts + teams,)),
+            dma((cuts + teams,)),
+            dma((cuts + 5,)),
+            dma((11,)),
             dma((teams, groups, pieces)),
             dma((teams, groups, pieces)),
-            dma((teams, local, groups, pieces)),
-            dma((teams, local, groups, pieces)),
+            dma((teams, groups, pieces)),
+            dma((teams, groups, pieces)),
             dma((teams, pieces)),
             dma((teams, pieces)),
             dma((groups,)),
@@ -882,7 +922,7 @@
             dma((peers,)),
         ],
         compiler_params=pltpu.CompilerParams(
-            collective_id=0, has_side_effects=True, vmem_limit_bytes=63 << 20
+            collective_id=0, has_side_effects=True, vmem_limit_bytes=62 << 20
         ),
     )(
         pad(norm_gain).reshape(1, wide),

time: 101 us -> 94.3 us (0.934)
  Pallas kernels: 96.6 us -> 91.9 us
  local copies, waits for them, and re-layouts: 3.76 us -> 1.59 us
    pallas_call x1, Pallas kernels: 96.6 us -> 91.9 us  [shards(): pl.pallas_call(functools.partial(layer_kernel, 8, pieces, slots), out_sha...]
    unnamed x2, local copies, waits for them, and re-layouts: 3.76 us -> 1.59 us
where the time goes in v3:
time: 94.3 us; the launch traced here: 94.1 us
  Pallas kernels  91.9 us (97%)
  local copies, waits for them, and re-layouts  1.59 us (2%)
    pallas_call x1, Pallas kernels, shards(): pl.pallas_call(functools.partial(layer_kernel, 8, pieces, slots), out_sha...  91.9 us

profile of v3, /device:TPU:0, one launch (start us, length us, event | category | flops | bytes accessed | tf_op | source)
XLA Modules:
  0.0 94.1 jit_solution(15670536062784949471)
XLA Ops:
  0.6 91.9 %shard_map.185 = (bf16[128,2048]{1,0:T(8,128)(2,1)S(1)}, bf16[128,2048]{1,0:T(8,128)(2,1)S(1)}) custom-call(f32[1,128]{1,0:T(1,128)} %bitcast.13, bf16[128,2048]{1,0:T(8,128)(2,1)} %x_in.1, f32[1,2048]{1,0:T(1,128)} %bitcast.10, s32[2,128]{1,0:T(2,128)} %bitcast.11, f32[2,128]{1,0:T(2,128)} %bitcast.12, bf16[1024,128]{1,0:T(8,128)(2,1)} %r_in.1, ...), custom_call_target="tpu_custom_call" | custom-call | tf_op jit(solution)/shard_map/pallas_call | solution.py:859
  92.5 0.8 copy.22
  93.3 0.8 copy.23

commit v4 on v3

--- a/solution.py
+++ b/solution.py
@@ -403,8 +403,8 @@
         return remote(
             leaving.at[s, q, :, cols],
             arrived.at[s, q, :, cols],
-            go_send.at[s, q, n],
-            go_recv.at[s, q, n],
+            go_send.at[s],
+            go_recv.at[s],
             column(q),
         )
 
@@ -413,9 +413,35 @@
         return remote(
             arrived.at[s, q, :, cols],
             returned.at[s, q, :, cols],
-            back_send.at[s, q, n],
-            back_recv.at[s, q, n],
+            back_send.at[s],
+            back_recv.at[s, n],
             column(-q),
+        )
+
+    others_of = pl.ds(1, groups - 1)
+
+    def go_all(s):
+        return remote(
+            leaving.at[s, others_of], arrived.at[s, others_of], go_send.at[s], go_recv.at[s], column(1)
+        )
+
+    def back_all(s):
+        return remote(
+            arrived.at[s, others_of],
+            returned.at[s, others_of],
+            back_send.at[s],
+            back_recv.at[s, 0],
+            column(1),
+        )
+
+    def back_piece(s, n):
+        cols = pl.ds(pl.multiple_of(n * piece, piece), piece)
+        return remote(
+            arrived.at[s, others_of, :, cols],
+            returned.at[s, others_of, :, cols],
+            back_send.at[s],
+            back_recv.at[s, n],
+            column(1),
         )
 
     def part_copy(s, n):
@@ -498,12 +524,16 @@
     for s in range(1, teams):
         for copy in table_copies(s):
             copy.start()
+    early = 1
+    for a in range(early):
+        pair_copy(a).start()
+    for s in range(1, teams):
         for n in range(pieces):
             token_copy(s, n).start()
     for s in range(teams):
         slab_copy(s).start()
     for a in range(cuts + 1):
-        if a < cuts:
+        if early <= a < cuts:
             pair_copy(a).start()
         core_copy(a).start()
         own_copy(a).start()
@@ -662,14 +692,7 @@
         lax.fori_loop(1, groups, back, 0)
 
     def come(s):
-        def each(q, carry):
-            def some(n, inner):
-                go_copy(s, q, n).wait_recv()
-                return inner
-
-            return lax.fori_loop(0, pieces, some, carry)
-
-        lax.fori_loop(1, groups, each, 0)
+        go_all(s).wait_recv()
 
     for a in range(firsts):
         relay(a)
@@ -704,14 +727,14 @@
             return carry
 
         lax.fori_loop(1, teams, mates, 0)
+        if n == 0:
+            enlarge(0, 0)
         if n == pieces // 2:
             for s in range(1, teams):
                 widened(s, bits - 1)
                 pair_copy(cuts + s).start()
                 core_copy(cuts + s).start()
 
-    enlarge(0, 0)
-
     def mine_too(n, carry):
         reduce(0, n)
         return carry
@@ -720,11 +743,7 @@
     widened(0, bits - 1)
     relay_copy(cuts).start()
     def combined(s, n):
-        def each(q, carry):
-            back_copy(s, q, n).wait_recv()
-            return carry
-
-        lax.fori_loop(1, groups, each, 0)
+        back_piece(s, n).wait_recv()
         cols = pl.ds(pl.multiple_of(n * piece, piece), piece)
         rows = returned[s, :, :, cols].reshape(groups * span, piece)
         return jnp.dot(spread_ref[s], rows, preferred_element_type=f32), cols
@@ -782,15 +801,9 @@
         ep_copy(q, here).wait_send()
 
     def sent(s, carry):
-        def each(q, inner):
-            def block(n, last):
-                go_copy(s, q, n).wait_send()
-                back_copy(s, q, n).wait_send()
-                return last
-
-            return lax.fori_loop(0, pieces, block, inner)
-
-        return lax.fori_loop(1, groups, each, carry)
+        go_all(s).wait_send()
+        back_all(s).wait_send()
+        return carry
 
     lax.fori_loop(0, teams, sent, 0)
 
@@ -910,10 +923,10 @@
             dma((cuts + teams,)),
             dma((cuts + 5,)),
             dma((11,)),
-            dma((teams, groups, pieces)),
-            dma((teams, groups, pieces)),
-            dma((teams, groups, pieces)),
-            dma((teams, groups, pieces)),
+            dma((teams,)),
+            dma((teams,)),
+            dma((teams,)),
+            dma((teams, pieces)),
             dma((teams, pieces)),
             dma((teams, pieces)),
             dma((groups,)),

time: 94.3 us -> 93.1 us (0.987)
  Pallas kernels: 91.9 us -> 90.7 us
    pallas_call x1, Pallas kernels: 91.9 us -> 90.7 us  [shards(): pl.pallas_call(functools.partial(layer_kernel, 8, pieces, slots), out_sha...]
where the time goes in v4:
time: 93.1 us; the launch traced here: 92.9 us
  Pallas kernels  90.7 us (97%)
  local copies, waits for them, and re-layouts  1.59 us (2%)
    pallas_call x1, Pallas kernels, shards(): pl.pallas_call(functools.partial(layer_kernel, 8, pieces, slots), out_sha...  90.7 us

profile of v4, /device:TPU:0, one launch (start us, length us, event | category | flops | bytes accessed | tf_op | source)
XLA Modules:
  0.0 92.9 jit_solution(11965084880193147165)
XLA Ops:
  0.6 90.7 %shard_map.185 = (bf16[128,2048]{1,0:T(8,128)(2,1)S(1)}, bf16[128,2048]{1,0:T(8,128)(2,1)S(1)}) custom-call(f32[1,128]{1,0:T(1,128)} %bitcast.13, bf16[128,2048]{1,0:T(8,128)(2,1)} %x_in.1, f32[1,2048]{1,0:T(1,128)} %bitcast.10, s32[2,128]{1,0:T(2,128)} %bitcast.11, f32[2,128]{1,0:T(2,128)} %bitcast.12, bf16[1024,128]{1,0:T(8,128)(2,1)} %r_in.1, ...), custom_call_target="tpu_custom_call" | custom-call | tf_op jit(solution)/shard_map/pallas_call | solution.py:872
  91.4 0.8 copy.22
  92.2 0.8 copy.23
